TPU v7x, 1024 devices: a whole 8x8x8 slice. The times are simulated.
1024 devices in a mesh: ep: 64 (over z, y), tp: 16 (over x, core).
Axes of the slice: x: 8, y: 8, z: 8, core: 2. Of those that a mesh axis runs over, the one named last changes fastest.
Arguments:
- tokens: bfloat16 [8192, 2048], P('ep'), may hold values from -6 to 6
- cotangent: bfloat16 [8192, 2048], P('ep'), may hold values from -0.796875 to 0.796875
- mix_weights: bfloat16 [8192, 2], P('ep'), may hold values from 0.049804688 to 1
- routes: int32 [8192, 2], P('ep'), may hold values from 0 to 63, all different within a row; in each aligned block of 128 rows (0 to 127, 128 to 255, ...) at most 5 rows name the same one
- gate_proj: bfloat16 [64, 2048, 2048], P('ep', None, 'tp'), may hold values from -0.125 to 0.125
- up_proj: bfloat16 [64, 2048, 2048], P('ep', None, 'tp'), may hold values from -0.125 to 0.125
- down_proj: bfloat16 [64, 2048, 2048], P('ep', 'tp'), may hold values from -0.125 to 0.125
Outputs:
- token_grad: bfloat16 [8192, 2048], P('ep', 'tp')
- mix_grad: bfloat16 [8192, 2], P('ep')
- gate_grad: bfloat16 [64, 2048, 2048], P('ep', None, 'tp')
- up_grad: bfloat16 [64, 2048, 2048], P('ep', None, 'tp')
- down_grad: bfloat16 [64, 2048, 2048], P('ep', 'tp')
Inputs may be any that keep to these rules, and one draw needn't show every extreme that they name: `routes`: each row names 2 different experts; in each aligned block of 128 rows (the rows of one device) no expert is named more than 5 times, a bound that some block reaches.
All inputs are finite; a program needn't handle non-finite values.
Results may differ from a plain program's by a relative error of at most 0.018.
Values may be sent and summed in bfloat16 or wider, within the bound.
No kernel may reach another device: no remote copies, remote signals or barrier semaphores. Data moves between devices by JAX's collectives and lax.ppermute only.
A program may use at most 128 MiB of HBM per device.

v0:
```python
import math

import jax
import jax.numpy as jnp
from jax import lax
from jax.sharding import PartitionSpec as P


def sent_together(arrays, axis, split_dim, concat_dim, along):
    widths = [math.prod(a.shape[along:]) for a in arrays]
    both = jnp.concatenate(
        [a.reshape(*a.shape[:along], w) for a, w in zip(arrays, widths)], axis=along
    )
    whole = lax.all_to_all(both, axis, split_axis=split_dim, concat_axis=concat_dim, tiled=True)
    pieces = jnp.split(whole, [sum(widths[:k]) for k in range(1, len(widths))], axis=along)
    return tuple(
        (b.reshape(*whole.shape[:along], *a.shape[along:]) for a, b in zip(arrays, pieces))
    )


def laid_out(pieces, dim):
    dims = list(pieces.shape[1:])
    dims[dim] *= pieces.shape[0]
    return jnp.moveaxis(pieces, 0, dim).reshape(dims)


def from_everyone(value, axis):
    copies = jnp.broadcast_to(value, (lax.axis_size(axis), *value.shape))
    return lax.all_to_all(copies, axis, split_axis=0, concat_axis=0, tiled=True)


def gathered_copies(value, axis, dim):
    return laid_out(from_everyone(value, axis), dim)


def in_one_piece(arrays, axis, dim, along):
    both = jnp.concatenate(arrays, axis=along)
    whole, at, done = (gathered_copies(both, axis, dim), 0, [])
    for a in arrays:
        done.append(lax.slice_in_dim(whole, at, at + a.shape[along], axis=along))
        at += a.shape[along]
    return tuple(done)


def over_copies(value, axis):
    return from_everyone(value, axis).sum(axis=0)


def cut_along(value, dim, devices):
    before, after = (value.shape[:dim], value.shape[dim + 1 :])
    return jnp.moveaxis(value.reshape(*before, devices, -1, *after), dim, 0)


def sent_and_summed(value, axis, dim):
    devices = lax.axis_size(axis)
    pieces = lax.all_to_all(cut_along(value, dim, devices), axis, 0, 0, tiled=True)
    return jnp.sum(pieces.astype(jnp.float32), axis=0)


def silu_slope(pre):
    sig = jax.nn.sigmoid(pre)
    return sig * (1.0 + pre * (1.0 - sig))


def place_rows(source, target, owner, experts, slots):
    filled = (
        jnp.zeros((experts * slots, source.shape[1]), source.dtype).at[target].set(source[owner])
    )
    return filled.reshape(experts, slots, source.shape[1])


def on_device(tokens, cotangent, mix_weights, routes, gate_proj, up_proj, down_proj):
    experts = lax.axis_size("ep")
    lanes = lax.axis_size("tp")
    tok_rows, width = tokens.shape
    top = routes.shape[1]
    slots = 5 * tok_rows * top // (4 * experts)
    flat = routes.reshape(-1)
    onehot = (flat[:, None] == jnp.arange(experts, dtype=jnp.int32)[None, :]).astype(jnp.int32)
    before = jnp.cumsum(onehot, axis=0) - onehot
    rank = jnp.sum(before * onehot, axis=1)
    target = flat * slots + rank
    owner = jnp.arange(tok_rows * top, dtype=jnp.int32) // top
    mix_slots = (
        jnp.zeros((experts * slots,), jnp.bfloat16)
        .at[target]
        .set(mix_weights.reshape(-1))
        .reshape(experts, slots)
    )
    share = width // lanes
    start = lax.axis_index("tp") * share
    token_part = lax.dynamic_slice_in_dim(tokens, start, share, 1)
    back_part = lax.dynamic_slice_in_dim(cotangent, start, share, 1)
    row_part, grad_part, mix_in = sent_together(
        (
            place_rows(token_part, target, owner, experts, slots),
            place_rows(back_part, target, owner, experts, slots),
            mix_slots,
        ),
        "ep",
        0,
        0,
        2,
    )
    rows, backs = in_one_piece((row_part, grad_part), "tp", 2, 0)
    count = experts * slots
    rows = rows.reshape(count, width)
    backs = backs.reshape(count, width)
    weight = mix_in.reshape(count, 1).astype(jnp.float32)
    gate_w = gate_proj[0]
    up_w = up_proj[0]
    down_w = down_proj[0]
    pre_gate = jnp.dot(rows, gate_w, preferred_element_type=jnp.float32)
    pre_up = jnp.dot(rows, up_w, preferred_element_type=jnp.float32)
    active = jax.nn.silu(pre_gate)
    hidden = (active * pre_up).astype(jnp.bfloat16)
    back_hidden = lax.dot_general(
        backs, down_w, (((1,), (1,)), ((), ())), preferred_element_type=jnp.float32
    )
    mix_part = jnp.sum(hidden.astype(jnp.float32) * back_hidden, axis=1).reshape(experts, slots)
    pair_mix = over_copies(mix_part, "tp").astype(jnp.bfloat16)
    weighted = (weight * hidden.astype(jnp.float32)).astype(jnp.bfloat16)
    down_grad = lax.dot_general(
        weighted, backs, (((0,), (0,)), ((), ())), preferred_element_type=jnp.float32
    ).astype(jnp.bfloat16)
    scaled = weight * back_hidden
    back_gate = (scaled * pre_up * silu_slope(pre_gate)).astype(jnp.bfloat16)
    back_up = (scaled * active).astype(jnp.bfloat16)
    gate_grad = lax.dot_general(
        rows, back_gate, (((0,), (0,)), ((), ())), preferred_element_type=jnp.float32
    ).astype(jnp.bfloat16)
    up_grad = lax.dot_general(
        rows, back_up, (((0,), (0,)), ((), ())), preferred_element_type=jnp.float32
    ).astype(jnp.bfloat16)
    partial_value = lax.dot_general(
        back_gate, gate_w, (((1,), (1,)), ((), ())), preferred_element_type=jnp.float32
    )
    partial_value = partial_value + lax.dot_general(
        back_up, up_w, (((1,), (1,)), ((), ())), preferred_element_type=jnp.float32
    )
    partial_value = partial_value.astype(jnp.bfloat16).astype(jnp.float32)
    pair_grad = sent_and_summed(
        partial_value.reshape(experts, slots, width).astype(jnp.bfloat16), "tp", 2
    ).astype(jnp.bfloat16)
    grad_back, mix_back = sent_together((pair_grad, pair_mix), "ep", 0, 0, 2)
    columns = grad_back.shape[2]
    picked = grad_back.reshape(count, columns)[target].astype(jnp.float32)
    token_grad = jnp.sum(picked.reshape(tok_rows, top, columns), axis=1).astype(jnp.bfloat16)
    mix_grad = mix_back.reshape(count)[target].reshape(tok_rows, top)
    return (token_grad, mix_grad, gate_grad[None], up_grad[None], down_grad[None])


def solution(mesh):
    in_specs = (
        P("ep", None),
        P("ep", None),
        P("ep", None),
        P("ep", None),
        P("ep", None, "tp"),
        P("ep", None, "tp"),
        P("ep", "tp", None),
    )
    out_specs = (
        P("ep", "tp"),
        P("ep", None),
        P("ep", None, "tp"),
        P("ep", None, "tp"),
        P("ep", "tp", None),
    )
    return jax.shard_map(
        on_device, mesh=mesh, in_specs=in_specs, out_specs=out_specs, check_vma=False
    )
```

profile of v0, /device:TPU:1, one launch (start us, length us, event | category | flops | bytes accessed | tf_op | source)
XLA Modules:
  0.0 203.6 jit_solution(4394051726563113514)
XLA Ops:
  0.7 0.8 copy.53
  1.8 0.7 broadcast_multiply_fusion
  2.5 0.6 reduce-window.6
  3.1 0.2 slice_reduce_fusion.1
  3.7 0.8 constant_dynamic-slice_fusion
  4.5 1.8 scatter_custom_fusion
  6.4 1.8 scatter_custom_fusion.1
  8.5 2.2 %scatter_custom_fusion.2 = bf16[320]{0:T(512)(128)(2,1)S(1)} fusion(s32[256]{0:T(256)S(1)} %bitcast.96, bf16[256]{0:T(256)(128)(2,1)S(1)} %reshape.214, bf16[]{:T(256)} %constant.20.clone.1), kind=kCustom, calls=%fused_computation.77 | custom fusion | bytes 642 | tf_op jit(solution)/shard_map/scatter | solution.py:87
  10.7 0.3 reshape_reshape.9
  11.0 38.8 %all_to_all.25 = bf16[64,5,257]{2,1,0:T(8,128)(2,1)S(1)} all-to-all(bf16[64,5,257]{2,1,0:T(8,128)(2,1)S(1)} %pad_maximum_fusion), channel_id=1, replica_groups=mesh['ep'=64,'tp'=16] {'ep'}, dimensions={0} | all-to-all | bytes 328960 | tf_op jit(solution)/shard_map/all_to_all | solution.py:14
  50.0 2.1 %broadcast_in_dim.13 = bf16[16,128,5,128]{3,1,2,0:T(8,128)(2,1)} broadcast(bf16[128,5,128]{2,0,1:T(8,128)(2,1)S(1)} %copy.58), dimensions={1,2,3} | broadcast | bytes 2785280 | tf_op jit(solution)/shard_map/broadcast_in_dim | solution.py:28
  52.1 10.0 %all-to-all-start.1 = ((bf16[16,128,5,128]{3,1,2,0:T(8,128)(2,1)}), bf16[16,128,5,128]{3,1,2,0:T(8,128)(2,1)S(1)}, u32[]{:S(2)}, u32[]{:S(2)}) async-start(bf16[16,128,5,128]{3,1,2,0:T(8,128)(2,1)} %broadcast_in_dim.13), calls=%async_computation.1 | async-start | bytes 5242880 | tf_op jit(solution)/shard_map/all_to_all | solution.py:29
  62.1 0.8 convert_reduce_fusion
  62.9 0.9 reshape.161
  63.8 57.9 %all-to-all-done.1 = bf16[16,128,5,128]{3,1,2,0:T(8,128)(2,1)S(1)} async-done(((bf16[16,128,5,128]{3,1,2,0:T(8,128)(2,1)}), bf16[16,128,5,128]{3,1,2,0:T(8,128)(2,1)S(1)}, u32[]{:S(2)}, u32[]{:S(2)}) %all-to-all-start.1) | async-done | bytes 2621472 | tf_op jit(solution)/shard_map/all_to_all | solution.py:29
  121.7 0.6 fusion.43
  122.3 0.8 copy.60
  123.2 0.5 fusion.7
  123.7 0.9 copy-done.5
  124.6 0.5 fusion.9
  125.1 0.8 copy.59
  126.0 0.2 copy-done.7
  126.1 0.6 fusion.26
  126.7 0.3 copy-done.1
  127.0 0.5 fusion.20
  127.7 0.7 reshape.235
  128.5 5.5 %all-to-all-start.3 = ((f32[16,1,320]{2,1,0:T(1,128)}), f32[16,1,320]{2,1,0:T(1,128)S(1)}, u32[]{:S(2)}, u32[]{:S(2)}) async-start(f32[16,1,320]{2,1,0:T(1,128)} %reshape.235), calls=%async_computation.3 | async-start | bytes 49152 | tf_op jit(solution)/shard_map/all_to_all | solution.py:29
  134.0 1.5 fusion.4
  135.6 0.3 copy.70
  135.9 1.4 copy.99
  137.3 4.1 %all-to-all-done.3 = f32[16,1,320]{2,1,0:T(1,128)S(1)} async-done(((f32[16,1,320]{2,1,0:T(1,128)}), f32[16,1,320]{2,1,0:T(1,128)S(1)}, u32[]{:S(2)}, u32[]{:S(2)}) %all-to-all-start.3) | async-done | bytes 20512 | tf_op jit(solution)/shard_map/all_to_all | solution.py:29
  141.4 4.0 %all-to-all-start.2 = ((bf16[16,64,5,128]{3,1,2,0:T(8,128)(2,1)}), bf16[16,64,5,128]{3,1,2,0:T(8,128)(2,1)S(1)}, u32[]{:S(2)}, u32[]{:S(2)}) async-start(bf16[16,64,5,128]{3,1,2,0:T(8,128)(2,1)} %bitcast.82), calls=%async_computation.2 | async-start | bytes 2621440 | tf_op jit(solution)/shard_map/all_to_all | solution.py:56
  145.4 1.5 fusion.2
  146.9 1.5 fusion.1
  148.4 0.5 broadcast.152
  148.9 0.7 reduce.8
  149.7 0.2 copy.64
  149.9 28.8 %all-to-all-done.2 = bf16[16,64,5,128]{3,1,2,0:T(8,128)(2,1)S(1)} async-done(((bf16[16,64,5,128]{3,1,2,0:T(8,128)(2,1)}), bf16[16,64,5,128]{3,1,2,0:T(8,128)(2,1)S(1)}, u32[]{:S(2)}, u32[]{:S(2)}) %all-to-all-start.2) | async-done | bytes 1310752 | tf_op jit(solution)/shard_map/all_to_all | solution.py:56
  178.7 0.3 reduce_sum.55
  179.0 0.8 pad_maximum_fusion.2
  179.8 4.6 %all-to-all-start.4 = ((bf16[64,5,129]{2,1,0:T(8,128)(2,1)}), bf16[64,5,129]{2,1,0:T(8,128)(2,1)S(1)}, u32[]{:S(2)}, u32[]{:S(2)}) async-start(bf16[64,5,129]{2,1,0:T(8,128)(2,1)} %pad_maximum_fusion.2), calls=%async_computation.4 | async-start | bytes 524288 | tf_op jit(solution)/shard_map/all_to_all | solution.py:14
  184.4 1.4 fusion.3
  185.8 13.1 %all-to-all-done.4 = bf16[64,5,129]{2,1,0:T(8,128)(2,1)S(1)} async-done(((bf16[64,5,129]{2,1,0:T(8,128)(2,1)}), bf16[64,5,129]{2,1,0:T(8,128)(2,1)S(1)}, u32[]{:S(2)}, u32[]{:S(2)}) %all-to-all-start.4) | async-done | bytes 82592 | tf_op jit(solution)/shard_map/all_to_all | solution.py:14
  198.9 0.2 slice_reduce_fusion
  199.2 1.9 gather_fusion.1
  201.3 0.6 copy.65
  202.0 0.9 gather_fusion
  202.9 0.8 reduce_sum.58
  (43 shorter events, 2.1 us)
Async XLA Ops:
  0.6 122.5 %copy-start = (bf16[1,2048,128]{2,1,0:T(8,128)(2,1)S(1)}, bf16[1,2048,128]{2,1,0:T(8,128)(2,1)}, u32[]{:S(2)}) copy-start(bf16[1,2048,128]{2,1,0:T(8,128)(2,1)} %param.11) | copy-start | bytes 1572868
  0.6 7.6 %copy-start.6 = (bf16[128,2]{0,1:T(2,128)(2,1)S(1)}, bf16[128,2]{0,1:T(2,128)(2,1)}, u32[]{:S(2)}) copy-start(bf16[128,2]{0,1:T(2,128)(2,1)} %param.9) | copy-start | bytes 1540
  52.1 69.6 %all-to-all-start.1 = ((bf16[16,128,5,128]{3,1,2,0:T(8,128)(2,1)}), bf16[16,128,5,128]{3,1,2,0:T(8,128)(2,1)S(1)}, u32[]{:S(2)}, u32[]{:S(2)}) async-start(bf16[16,128,5,128]{3,1,2,0:T(8,128)(2,1)} %broadcast_in_dim.13), calls=%async_computation.1 | async-start | bytes 5242880 | tf_op jit(solution)/shard_map/all_to_all | solution.py:29
  123.1 1.9 copy-start.3
  123.1 1.4 copy-start.5
  125.1 1.0 copy-start.7
  126.0 1.1 copy-start.1
  128.5 12.9 %all-to-all-start.3 = ((f32[16,1,320]{2,1,0:T(1,128)}), f32[16,1,320]{2,1,0:T(1,128)S(1)}, u32[]{:S(2)}, u32[]{:S(2)}) async-start(f32[16,1,320]{2,1,0:T(1,128)} %reshape.235), calls=%async_computation.3 | async-start | bytes 49152 | tf_op jit(solution)/shard_map/all_to_all | solution.py:29
  141.4 4.0 %copy-start.4 = (bf16[64,5,16,128]{3,2,1,0:T(8,128)(2,1)S(1)}, bf16[64,5,16,128]{3,2,1,0:T(8,128)(2,1)}, u32[]{:S(2)}) copy-start(bf16[64,5,16,128]{3,2,1,0:T(8,128)(2,1)} %copy-done.3) | copy-start | bytes 3932164
  141.4 37.3 %all-to-all-start.2 = ((bf16[16,64,5,128]{3,1,2,0:T(8,128)(2,1)}), bf16[16,64,5,128]{3,1,2,0:T(8,128)(2,1)S(1)}, u32[]{:S(2)}, u32[]{:S(2)}) async-start(bf16[16,64,5,128]{3,1,2,0:T(8,128)(2,1)} %bitcast.82), calls=%async_computation.2 | async-start | bytes 2621440 | tf_op jit(solution)/shard_map/all_to_all | solution.py:56
  149.9 34.6 %copy-start.2 = (bf16[64,5,16,128]{3,2,1,0:T(8,128)(2,1)S(1)}, bf16[64,5,16,128]{3,2,1,0:T(8,128)(2,1)}, u32[]{:S(2)}) copy-start(bf16[64,5,16,128]{3,2,1,0:T(8,128)(2,1)} %copy-done.1) | copy-start | bytes 3932164
  179.8 19.1 %all-to-all-start.4 = ((bf16[64,5,129]{2,1,0:T(8,128)(2,1)}), bf16[64,5,129]{2,1,0:T(8,128)(2,1)S(1)}, u32[]{:S(2)}, u32[]{:S(2)}) async-start(bf16[64,5,129]{2,1,0:T(8,128)(2,1)} %pad_maximum_fusion.2), calls=%async_computation.4 | async-start | bytes 524288 | tf_op jit(solution)/shard_map/all_to_all | solution.py:14
where the time goes:
time: 204 us
  waiting for transfers between devices  104 us (51%)
  blocking collectives  38.8 us (19%)
  starting transfers between devices  24.2 us (12%)
  local copies, waits for them, and re-layouts  22.8 us (11%)
  matrix products  7.98 us (4%)
  other arithmetic  4.91 us (2%)
    all_to_all x2, waiting for transfers between devices, from_everyone(): return lax.all_to_all(copies, axis, split_axis=0, concat_axis=0, tiled=True)  62 us
    all_to_all x1, blocking collectives, sent_together(): lax.all_to_all(both, axis, split_axis=split_dim, concat_axis=concat_dim,...  38.8 us
    all_to_all x1, waiting for transfers between devices, sent_and_summed(): lax.all_to_all(cut_along(value, dim, devices), axis, 0, 0, tiled=True)  28.8 us
    all_to_all x2, starting transfers between devices, from_everyone(): return lax.all_to_all(copies, axis, split_axis=0, concat_axis=0, tiled=True)  15.6 us
    all_to_all x1, waiting for transfers between devices, sent_together(): lax.all_to_all(both, axis, split_axis=split_dim, concat_axis=concat_dim,...  13.1 us
    all_to_all x1, starting transfers between devices, sent_together(): lax.all_to_all(both, axis, split_axis=split_dim, concat_axis=concat_dim,...  4.61 us
    unnamed x24, local copies, waits for them, and re-layouts  4.11 us
  transfers between devices with their start and end apart: 4, of which 4 were waited for; matrix products, arithmetic and copies ran while one was open for 5% of the time, Pallas kernels for 0%

commit v1 on v0

v1 whole, which is shorter than its diff:
```python
import jax
import jax.numpy as jnp
from jax import lax
from jax.sharding import Mesh
from jax.sharding import PartitionSpec as P

SLOTS = 5
LANES = 128


def silu_slope(pre):
    sig = jax.nn.sigmoid(pre)
    return sig * (1.0 + pre * (1.0 - sig))


def swap_cores(value):
    return lax.ppermute(value, "c", [(0, 1), (1, 0)])


def on_device(tokens, cotangent, mix_weights, routes, gate_proj, up_proj, down_proj):
    experts = lax.axis_size("ep")
    chips = lax.axis_size("x")
    core = lax.axis_index("c")
    tok_rows, width = tokens.shape
    top = routes.shape[1]
    count = experts * SLOTS
    half = width // 2
    f32 = jnp.float32
    bf16 = jnp.bfloat16

    flat = routes.T.reshape(-1)
    onehot = (flat[:, None] == jnp.arange(experts, dtype=jnp.int32)[None, :]).astype(bf16)
    pairs = tok_rows * top
    order = jnp.arange(pairs, dtype=jnp.int32)
    earlier = (order[:, None] > order[None, :]).astype(bf16)
    before = jnp.dot(earlier, onehot, preferred_element_type=f32)
    rank = jnp.sum(before * onehot.astype(f32), axis=1).astype(jnp.int32)
    target = (flat * SLOTS + rank).reshape(top, tok_rows)

    slot_ids = jnp.arange(count, dtype=jnp.int32)[:, None]
    place = jnp.zeros((count, tok_rows), bf16)
    place_mix = jnp.zeros((count, tok_rows), bf16)
    for k in range(top):
        hit = slot_ids == target[k][None, :]
        place = jnp.where(hit, jnp.asarray(1.0, bf16), place)
        place_mix = jnp.where(hit, mix_weights[:, k][None, :], place_mix)

    tok_half = lax.dynamic_slice_in_dim(tokens, core * half, half, 1)
    back_half = lax.dynamic_slice_in_dim(cotangent, core * half, half, 1)
    send_tok = jnp.dot(place, tok_half, preferred_element_type=f32).astype(bf16)
    send_back = jnp.dot(place_mix, back_half, preferred_element_type=f32).astype(bf16)
    tiles = half // LANES
    send = jnp.concatenate(
        [
            send_tok.reshape(experts, SLOTS * tiles, LANES),
            send_back.reshape(experts, SLOTS * tiles, LANES),
        ],
        axis=1,
    )
    got = lax.all_to_all(send, "ep", 0, 0, tiled=True)
    own_rows = got[:, : SLOTS * tiles].reshape(count, half)
    own_backs = got[:, SLOTS * tiles :].reshape(count, half)
    oth_rows = swap_cores(own_rows)
    oth_backs = swap_cores(own_backs)
    first = core == 0
    rows = jnp.concatenate(
        [jnp.where(first, own_rows, oth_rows), jnp.where(first, oth_rows, own_rows)], axis=1
    )
    backs = jnp.concatenate(
        [jnp.where(first, own_backs, oth_backs), jnp.where(first, oth_backs, own_backs)], axis=1
    )

    gate_w = gate_proj[0]
    up_w = up_proj[0]
    down_w = down_proj[0]
    pre_gate = jnp.dot(rows, gate_w, preferred_element_type=f32)
    pre_up = jnp.dot(rows, up_w, preferred_element_type=f32)
    active = jax.nn.silu(pre_gate)
    hidden = (active * pre_up).astype(bf16)
    scaled = lax.dot_general(backs, down_w, (((1,), (1,)), ((), ())), preferred_element_type=f32)
    mix_part = jnp.sum(hidden.astype(f32) * scaled, axis=1)
    back_gate = (scaled * pre_up * silu_slope(pre_gate)).astype(bf16)
    back_up = (scaled * active).astype(bf16)
    part = lax.dot_general(
        back_gate, gate_w, (((1,), (1,)), ((), ())), preferred_element_type=f32
    ) + lax.dot_general(back_up, up_w, (((1,), (1,)), ((), ())), preferred_element_type=f32)

    down_grad = lax.dot_general(
        hidden, backs, (((0,), (0,)), ((), ())), preferred_element_type=f32
    ).astype(bf16)
    gate_grad = lax.dot_general(
        rows, back_gate, (((0,), (0,)), ((), ())), preferred_element_type=f32
    ).astype(bf16)
    up_grad = lax.dot_general(
        rows, back_up, (((0,), (0,)), ((), ())), preferred_element_type=f32
    ).astype(bf16)

    mix_rows = jnp.pad(mix_part, (0, 8 * LANES - count)).reshape(1, 8, LANES)
    mix_rows = jnp.broadcast_to(mix_rows.astype(bf16), (chips, 8, LANES))
    part = part.astype(bf16).reshape(count, chips, 2, LANES)

    def for_core(which):
        piece = lax.dynamic_index_in_dim(part, which, 2, keepdims=False)
        return jnp.concatenate([jnp.moveaxis(piece, 1, 0), mix_rows], axis=1)

    theirs = swap_cores(for_core(1 - core))
    pair = (for_core(core).astype(f32) + theirs.astype(f32)).astype(bf16)
    pieces = lax.all_to_all(pair, "x", 0, 0, tiled=True)
    total = jnp.sum(pieces.astype(f32), axis=0).astype(bf16)
    grads = total[:count].reshape(experts, SLOTS, LANES)
    mixes = jnp.broadcast_to(total[count : count + 3][None], (experts, 3, LANES))
    back = lax.all_to_all(jnp.concatenate([grads, mixes], axis=1), "ep", 0, 0, tiled=True)

    flat_back = back.reshape(experts * 8, LANES)
    place8 = (flat * 8 + rank).reshape(top, tok_rows)
    cols = jnp.arange(experts * 8, dtype=jnp.int32)[None, :]
    pick = sum((place8[k][:, None] == cols).astype(bf16) for k in range(top))
    token_grad = jnp.dot(pick, flat_back, preferred_element_type=f32).astype(bf16)
    at = lax.axis_index("ep") * SLOTS + rank
    row8 = flat * 8 + SLOTS + at // LANES
    pick_mix = (row8[:, None] == cols).astype(bf16)
    mix_lines = jnp.dot(pick_mix, flat_back, preferred_element_type=f32)
    lane = (at % LANES)[:, None] == jnp.arange(LANES, dtype=jnp.int32)[None, :]
    mix_flat = jnp.sum(jnp.where(lane, mix_lines, 0.0), axis=1).reshape(top, tok_rows).T
    mix_grad = (mix_flat / mix_weights.astype(f32)).astype(bf16)
    return (token_grad, mix_grad, gate_grad[None], up_grad[None], down_grad[None])


def solution(mesh):
    ep = mesh.shape["ep"]
    split = Mesh(mesh.devices.reshape(ep, mesh.shape["tp"] // 2, 2), ("ep", "x", "c"))
    tp = ("x", "c")
    in_specs = (
        P("ep", None),
        P("ep", None),
        P("ep", None),
        P("ep", None),
        P("ep", None, tp),
        P("ep", None, tp),
        P("ep", tp, None),
    )
    out_specs = (
        P("ep", tp),
        P("ep", None),
        P("ep", None, tp),
        P("ep", None, tp),
        P("ep", tp, None),
    )
    return jax.shard_map(
        on_device, mesh=split, in_specs=in_specs, out_specs=out_specs, check_vma=False
    )
```

time: 204 us -> 133 us (0.65)
  waiting for transfers between devices: 104 us -> 29 us
  blocking collectives: 38.8 us -> 57.1 us
  local copies, waits for them, and re-layouts: 22.8 us -> 8.73 us
  matrix products: 7.98 us -> 11.6 us
  other arithmetic: 4.91 us -> 2.58 us
    all_to_all x4 -> x2, waiting for transfers between devices: 104 us -> 27.4 us  [the longest x1 19.7 us: on_device(): pieces = lax.all_to_all(pair, 'x', 0, 0, tiled=True)]
    all_to_all x1, blocking collectives: 38.8 us -> 57.1 us  [on_device(): got = lax.all_to_all(send, 'ep', 0, 0, tiled=True)]
    all_to_all x4 -> x2, starting transfers between devices: 24.2 us -> 13.2 us  [the longest x1 6.7 us: on_device(): lax.all_to_all(jnp.concatenate([grads, mixes], axis=1), 'ep', 0, 0, tiled...]
    ppermute x0 -> x3, starting transfers between devices: none -> 9.45 us  [swap_cores(): return lax.ppermute(value, 'c', [(0, 1), (1, 0)])]
    scatter x3 -> x0, local copies, waits for them, and re-layouts: 5.73 us -> none  [the longest x2 3.57 us: place_rows(): jnp.zeros((experts * slots, source.shape[1]), source.dtype).at[target]]
    dot_general x3 -> x8, matrix products: 2.37 us -> 7.15 us  [the longest x1 2.37 us: on_device(): lax.dot_general(hidden, backs, (((0,), (0,)), ((), ())), preferred_elemen...]
    gather x2 -> x0, local copies, waits for them, and re-layouts: 2.79 us -> none  [the longest x1 1.94 us: on_device(): mix_grad = mix_back.reshape(count)[target].reshape(tok_rows, top)]
    slice x4 -> x5, local copies, waits for them, and re-layouts: 2.44 us -> 0.13 us  [the longest x1 0.11 us: on_device(): own_rows = got[:, :SLOTS * tiles].reshape(count, half)]
  transfers between devices with their start and end apart: 4 -> 5, of which waited for: 4 -> 3; matrix products, arithmetic and copies ran while one was open for 5% -> 5% of each run, Pallas kernels for 0% -> 0%
where the time goes in v1:
time: 133 us
  blocking collectives  57.1 us (43%)
  waiting for transfers between devices  29 us (22%)
  starting transfers between devices  22.6 us (17%)
  matrix products  11.6 us (9%)
  local copies, waits for them, and re-layouts  8.73 us (7%)
  other arithmetic  2.58 us (2%)
    all_to_all x1, blocking collectives, on_device(): got = lax.all_to_all(send, 'ep', 0, 0, tiled=True)  57.1 us
    all_to_all x1, waiting for transfers between devices, on_device(): pieces = lax.all_to_all(pair, 'x', 0, 0, tiled=True)  19.7 us
    ppermute x3, starting transfers between devices, swap_cores(): return lax.ppermute(value, 'c', [(0, 1), (1, 0)])  9.45 us
    all_to_all x1, waiting for transfers between devices, on_device(): lax.all_to_all(jnp.concatenate([grads, mixes], axis=1), 'ep', 0, 0, tiled...  7.73 us
    all_to_all x1, starting transfers between devices, on_device(): lax.all_to_all(jnp.concatenate([grads, mixes], axis=1), 'ep', 0, 0, tiled...  6.7 us
    all_to_all x1, starting transfers between devices, on_device(): pieces = lax.all_to_all(pair, 'x', 0, 0, tiled=True)  6.49 us
    dynamic_slice x1, local copies, waits for them, and re-layouts, for_core(): piece = lax.dynamic_index_in_dim(part, which, 2, keepdims=False)  2.71 us
  transfers between devices with their start and end apart: 5, of which 3 were waited for; matrix products, arithmetic and copies ran while one was open for 5% of the time, Pallas kernels for 0%

profile of v1, /device:TPU:1, one launch (start us, length us, event | category | flops | bytes accessed | tf_op | source)
XLA Modules:
  0.0 132.7 jit_solution(16863427928807386319)
XLA Ops:
  0.6 0.0 copy-start
  0.7 1.0 fusion.5
  1.7 0.7 fusion.47
  2.4 0.7 slice_bitcast_fusion.1
  3.1 1.3 convolution_convert_fusion.3
  4.4 0.3 reshape.103
  4.7 0.3 convolution_convert_fusion.4
  5.0 0.3 reshape.102
  5.3 0.1 pad_maximum_fusion
  5.4 57.1 %all_to_all.15 = bf16[64,80,128]{2,1,0:T(8,128)(2,1)S(1)} all-to-all(bf16[64,80,128]{2,1,0:T(8,128)(2,1)S(1)} %pad_maximum_fusion), channel_id=1, replica_groups=mesh['ep'=64,'x'=8,'c'=2] {'ep'}, dimensions={0} | all-to-all | bytes 2621440 | tf_op jit(solution)/shard_map/all_to_all | solution.py:60
  62.5 0.1 fusion.57
  62.6 0.3 reshape.105
  62.9 5.1 %collective-permute-start.1 = (bf16[320,1024]{1,0:T(8,128)(2,1)S(1)}, bf16[320,1024]{1,0:T(8,128)(2,1)S(1)}, u32[]{:S(2)}, u32[]{:S(2)}) collective-permute-start(bf16[320,1024]{1,0:T(8,128)(2,1)S(1)} %reshape.105), channel_id=1, source_target_pairs={{0,1},{1,0},{2,3},{3,2},{4,5},{5,4},{6,7},{7,6},{8,9},{9,8},{10,11... | collective-permute-start | bytes 1966088 | tf_op jit(solution)/shard_map/ppermute | solution.py:17
  68.0 0.3 reshape.104
  68.3 1.9 %collective-permute-start = (bf16[320,1024]{1,0:T(8,128)(2,1)S(1)}, bf16[320,1024]{1,0:T(8,128)(2,1)S(1)}, u32[]{:S(2)}, u32[]{:S(2)}) collective-permute-start(bf16[320,1024]{1,0:T(8,128)(2,1)S(1)} %reshape.104), channel_id=1, source_target_pairs={{0,1},{1,0},{2,3},{3,2},{4,5},{5,4},{6,7},{7,6},{8,9},{9,8},{10,11... | collective-permute-start | bytes 1966088 | tf_op jit(solution)/shard_map/ppermute | solution.py:17
  70.2 0.1 broadcast_select_fusion.1
  70.4 0.0 copy-start.8
  70.4 0.5 fusion.9
  70.9 0.3 copy-done.1
  71.2 0.2 copy-done.3
  71.4 0.4 copy-done.8
  71.8 0.5 fusion.12
  72.3 0.1 broadcast_select_fusion.3
  72.5 0.9 copy-done.11
  73.4 0.6 multiply_reduce_fusion
  74.0 0.5 fusion.7
  74.5 0.5 fusion
  75.1 1.0 reshape.106
  76.0 2.7 %constant_dynamic-slice_fusion.1 = (bf16[320,8,1,128]{3,2,1,0:T(2,128)(2,1)S(1)}, bf16[320,8,1,128]{3,2,1,0:T(2,128)(2,1)S(1)}) fusion(bf16[320,8,2,128]{3,2,1,0:T(2,128)(2,1)S(1)} %reshape.106, s32[]{:T(128)S(6)} %select_n.79, s32[]{:T(128)S(6)} %select_n.80), kind=kLoop, calls=%fused_computation.86 | loop fusion | bytes 2621448 | tf_op jit(solution)/shard_map/jit(dynamic_index_in_dim)/dynamic_slice | solution.py:103
  78.7 0.1 copy.21
  78.8 0.1 pad_maximum_fusion.3
  78.9 2.4 %collective-permute-start.2 = (bf16[8,328,128]{2,0,1:T(8,128)(2,1)S(1)}, bf16[8,328,128]{2,0,1:T(8,128)(2,1)S(1)}, u32[]{:S(2)}, u32[]{:S(2)}) collective-permute-start(bf16[8,328,128]{2,0,1:T(8,128)(2,1)S(1)} %pad_maximum_fusion.3), channel_id=1, source_target_pairs={{0,1},{1,0},{2,3},{3,2},{4,5},{5,4},{6,7},{7,6},{8,9},{9,8},{10,11... | collective-permute-start | bytes 2015240 | tf_op jit(solution)/shard_map/ppermute | solution.py:17
  81.3 0.1 copy.22
  81.4 1.6 %collective-permute-done.2 = bf16[8,328,128]{2,0,1:T(8,128)(2,1)S(1)} collective-permute-done((bf16[8,328,128]{2,0,1:T(8,128)(2,1)S(1)}, bf16[8,328,128]{2,0,1:T(8,128)(2,1)S(1)}, u32[]{:S(2)}, u32[]{:S(2)}) %collective-permute-start.2) | collective-permute-done | bytes 671776 | tf_op jit(solution)/shard_map/ppermute | solution.py:17
  83.1 0.2 add_convert_fusion
  83.3 0.9 copy.16
  84.2 6.5 %all-to-all-start.1 = ((bf16[8,328,128]{2,1,0:T(8,128)(2,1)}), bf16[8,328,128]{2,1,0:T(8,128)(2,1)S(1)}, u32[]{:S(2)}, u32[]{:S(2)}) async-start(bf16[8,328,128]{2,1,0:T(8,128)(2,1)} %copy.16), calls=%async_computation.1 | async-start | bytes 1343488 | tf_op jit(solution)/shard_map/all_to_all | solution.py:108
  90.7 1.4 %fusion.2 = bf16[1,2048,128]{2,1,0:T(8,128)(2,1)} fusion(bf16[320,128]{1,0:T(8,128)(2,1)S(1)} %get-tuple-element.16, bf16[320,1024]{1,0:T(8,128)(2,1)S(1)} %copy-done.4, bf16[320,1024]{1,0:T(8,128)(2,1)S(1)} %copy-done.2), kind=kOutput, calls=%fused_computation.6 | convolution fusion | flops 170655744 | bytes 1916928 | tf_op jit(solution)/shard_map/dot_general | solution.py:94
  92.1 19.7 %all-to-all-done.1 = bf16[8,328,128]{2,1,0:T(8,128)(2,1)S(1)} async-done(((bf16[8,328,128]{2,1,0:T(8,128)(2,1)}), bf16[8,328,128]{2,1,0:T(8,128)(2,1)S(1)}, u32[]{:S(2)}, u32[]{:S(2)}) %all-to-all-start.1) | async-done | bytes 671776 | tf_op jit(solution)/shard_map/all_to_all | solution.py:108
  111.8 0.1 reduce_sum.41
  112.0 0.7 pad_maximum_fusion.7
  112.7 6.7 %all-to-all-start.2 = ((bf16[64,8,128]{2,1,0:T(8,128)(2,1)}), bf16[64,8,128]{2,1,0:T(8,128)(2,1)S(1)}, u32[]{:S(2)}, u32[]{:S(2)}) async-start(bf16[64,8,128]{2,1,0:T(8,128)(2,1)} %pad_maximum_fusion.7), calls=%async_computation.2 | async-start | bytes 262144 | tf_op jit(solution)/shard_map/all_to_all | solution.py:112
  119.4 2.4 %fusion.3 = bf16[1,128,2048]{2,1,0:T(8,128)(2,1)} fusion(bf16[320,128]{1,0:T(8,128)(2,1)S(1)} %get-tuple-element.6, bf16[320,1024]{1,0:T(8,128)(2,1)} %copy-done.7, bf16[320,1024]{1,0:T(8,128)(2,1)S(1)} %copy-done.6), kind=kOutput, calls=%fused_computation.7 | convolution fusion | flops 170655744 | bytes 1916928 | tf_op jit(solution)/shard_map/dot_general | solution.py:88
  121.8 1.4 %fusion.1 = bf16[1,2048,128]{2,1,0:T(8,128)(2,1)} fusion(bf16[320,128]{1,0:T(8,128)(2,1)S(1)} %get-tuple-element.15, bf16[320,1024]{1,0:T(8,128)(2,1)S(1)} %copy-done.4, bf16[320,1024]{1,0:T(8,128)(2,1)S(1)} %copy-done.2), kind=kOutput, calls=%fused_computation.5 | convolution fusion | flops 170655744 | bytes 1916928 | tf_op jit(solution)/shard_map/dot_general | solution.py:91
  123.2 7.7 %all-to-all-done.2 = bf16[64,8,128]{2,1,0:T(8,128)(2,1)S(1)} async-done(((bf16[64,8,128]{2,1,0:T(8,128)(2,1)}), bf16[64,8,128]{2,1,0:T(8,128)(2,1)S(1)}, u32[]{:S(2)}, u32[]{:S(2)}) %all-to-all-start.2) | async-done | bytes 131104 | tf_op jit(solution)/shard_map/all_to_all | solution.py:112
  131.0 0.3 fusion.4
  131.3 0.5 fusion.50
  131.8 0.9 convolution_convert_fusion.5
  (28 shorter events, 0.1 us)
Async XLA Ops:
  0.6 69.7 %copy-start = (bf16[1,2048,128]{2,1,0:T(8,128)(2,1)S(1)}, bf16[1,2048,128]{2,1,0:T(8,128)(2,1)}, u32[]{:S(2)}) copy-start(bf16[1,2048,128]{2,1,0:T(8,128)(2,1)} %param.11) | copy-start | bytes 1572868
  0.6 4.0 %copy-start.9 = (bf16[128,2048]{1,0:T(8,128)(2,1)S(1)}, bf16[128,2048]{1,0:T(8,128)(2,1)}, u32[]{:S(2)}) copy-start(bf16[128,2048]{1,0:T(8,128)(2,1)} %param.7) | copy-start | bytes 1572868
  62.9 7.4 %collective-permute-start.1 = (bf16[320,1024]{1,0:T(8,128)(2,1)S(1)}, bf16[320,1024]{1,0:T(8,128)(2,1)S(1)}, u32[]{:S(2)}, u32[]{:S(2)}) collective-permute-start(bf16[320,1024]{1,0:T(8,128)(2,1)S(1)} %reshape.105), channel_id=1, source_target_pairs={{0,1},{1,0},{2,3},{3,2},{4,5},{5,4},{6,7},{7,6},{8,9},{9,8},{10,11... | collective-permute-start | bytes 1966088 | tf_op jit(solution)/shard_map/ppermute | solution.py:17
  68.3 4.0 %collective-permute-start = (bf16[320,1024]{1,0:T(8,128)(2,1)S(1)}, bf16[320,1024]{1,0:T(8,128)(2,1)S(1)}, u32[]{:S(2)}, u32[]{:S(2)}) collective-permute-start(bf16[320,1024]{1,0:T(8,128)(2,1)S(1)} %reshape.104), channel_id=1, source_target_pairs={{0,1},{1,0},{2,3},{3,2},{4,5},{5,4},{6,7},{7,6},{8,9},{9,8},{10,11... | collective-permute-start | bytes 1966088 | tf_op jit(solution)/shard_map/ppermute | solution.py:17
  70.3 0.9 copy-start.1
  70.4 1.1 copy-start.3
  70.4 1.4 %copy-start.8 = (bf16[1,2048,128]{2,1,0:T(8,128)(2,1)S(1)}, bf16[1,2048,128]{2,1,0:T(8,128)(2,1)}, u32[]{:S(2)}) copy-start(bf16[1,2048,128]{2,1,0:T(8,128)(2,1)} %param.12) | copy-start | bytes 1572868
  72.3 1.1 copy-start.11
  72.4 1.6 %copy-start.5 = (bf16[320,1024]{1,0:T(8,128)(2,1)}, bf16[320,1024]{1,0:T(8,128)(2,1)S(1)}, u32[]{:S(2)}) copy-start(bf16[320,1024]{1,0:T(8,128)(2,1)S(1)} %get-tuple-element.13) | copy-start | bytes 1966084
  72.5 1.6 %copy-start.7 = (bf16[320,1024]{1,0:T(8,128)(2,1)}, bf16[320,1024]{1,0:T(8,128)(2,1)S(1)}, u32[]{:S(2)}) copy-start(bf16[320,1024]{1,0:T(8,128)(2,1)S(1)} %get-tuple-element.14) | copy-start | bytes 1966084
  78.9 4.1 %collective-permute-start.2 = (bf16[8,328,128]{2,0,1:T(8,128)(2,1)S(1)}, bf16[8,328,128]{2,0,1:T(8,128)(2,1)S(1)}, u32[]{:S(2)}, u32[]{:S(2)}) collective-permute-start(bf16[8,328,128]{2,0,1:T(8,128)(2,1)S(1)} %pad_maximum_fusion.3), channel_id=1, source_target_pairs={{0,1},{1,0},{2,3},{3,2},{4,5},{5,4},{6,7},{7,6},{8,9},{9,8},{10,11... | collective-permute-start | bytes 2015240 | tf_op jit(solution)/shard_map/ppermute | solution.py:17
  83.2 7.5 %copy-start.2 = (bf16[320,1024]{1,0:T(8,128)(2,1)S(1)}, bf16[320,1024]{1,0:T(8,128)(2,1)}, u32[]{:S(2)}) copy-start(bf16[320,1024]{1,0:T(8,128)(2,1)} %copy-done.1) | copy-start | bytes 1966084
  83.2 7.5 %copy-start.4 = (bf16[320,1024]{1,0:T(8,128)(2,1)S(1)}, bf16[320,1024]{1,0:T(8,128)(2,1)}, u32[]{:S(2)}) copy-start(bf16[320,1024]{1,0:T(8,128)(2,1)} %copy-done.3) | copy-start | bytes 1966084
  84.2 27.6 %all-to-all-start.1 = ((bf16[8,328,128]{2,1,0:T(8,128)(2,1)}), bf16[8,328,128]{2,1,0:T(8,128)(2,1)S(1)}, u32[]{:S(2)}, u32[]{:S(2)}) async-start(bf16[8,328,128]{2,1,0:T(8,128)(2,1)} %copy.16), calls=%async_computation.1 | async-start | bytes 1343488 | tf_op jit(solution)/shard_map/all_to_all | solution.py:108
  92.1 27.3 %copy-start.6 = (bf16[320,1024]{1,0:T(8,128)(2,1)S(1)}, bf16[320,1024]{1,0:T(8,128)(2,1)}, u32[]{:S(2)}) copy-start(bf16[320,1024]{1,0:T(8,128)(2,1)} %copy-done.5) | copy-start | bytes 1966084
  112.7 18.2 %all-to-all-start.2 = ((bf16[64,8,128]{2,1,0:T(8,128)(2,1)}), bf16[64,8,128]{2,1,0:T(8,128)(2,1)S(1)}, u32[]{:S(2)}, u32[]{:S(2)}) async-start(bf16[64,8,128]{2,1,0:T(8,128)(2,1)} %pad_maximum_fusion.7), calls=%async_computation.2 | async-start | bytes 262144 | tf_op jit(solution)/shard_map/all_to_all | solution.py:112
  121.8 9.5 %copy-start.10 = (bf16[128,2]{0,1:T(2,128)(2,1)S(1)}, bf16[128,2]{0,1:T(2,128)(2,1)}, u32[]{:S(2)}) copy-start(bf16[128,2]{0,1:T(2,128)(2,1)} %param.9) | copy-start | bytes 1540

commit v2 on v1

v2 whole, which is shorter than its diff:
```python
import jax
import jax.numpy as jnp
from jax import lax
from jax.experimental import pallas as pl
from jax.experimental.pallas import tpu as pltpu
from jax.sharding import Mesh
from jax.sharding import PartitionSpec as P

SLOTS = 5
LANES = 128
ROWS8 = 8
F32 = jnp.float32
BF16 = jnp.bfloat16


def iota(shape, dim):
    return lax.broadcasted_iota(jnp.int32, shape, dim)


def dot_nn(a, b):
    return lax.dot_general(a, b, (((1,), (0,)), ((), ())), preferred_element_type=F32)


def dot_nt(a, b):
    return lax.dot_general(a, b, (((1,), (1,)), ((), ())), preferred_element_type=F32)


def dot_tn(a, b):
    return lax.dot_general(a, b, (((0,), (0,)), ((), ())), preferred_element_type=F32)


def swap_cores(value):
    return lax.ppermute(value, "c", [(0, 1), (1, 0)])


def slots_of(routes, experts):
    tok = routes.shape[1]
    ids = iota((experts, tok), 0)
    named = [ids == routes[k : k + 1] for k in range(2)]
    both = jnp.where(named[0] | named[1], 1.0, 0.0).astype(BF16)
    earlier = jnp.where(iota((tok, tok), 0) < iota((tok, tok), 1), 1.0, 0.0).astype(BF16)
    before = dot_nn(both, earlier)
    return [
        jnp.sum(jnp.where(hit, before, 0.0), axis=0, keepdims=True).astype(jnp.int32)
        for hit in named
    ]


def dispatch_kernel(core_ref, routes_ref, mix_ref, tok_ref, cot_ref, send_ref):
    del core_ref
    routes = routes_ref[...]
    mix = mix_ref[...].astype(F32)
    count, _ = send_ref.shape
    experts = count // (2 * SLOTS)
    tok = routes.shape[1]
    ranks = slots_of(routes, experts)
    at = [routes[k : k + 1] * (2 * SLOTS) + ranks[k] for k in range(2)]
    row = iota((count, tok), 0)
    place = jnp.where((row == at[0]) | (row == at[1]), 1.0, 0.0)
    scale = jnp.where(
        row == at[0] + SLOTS, mix[0:1], jnp.where(row == at[1] + SLOTS, mix[1:2], 0.0)
    )
    pick = jnp.concatenate([place.astype(BF16), scale.astype(BF16)], axis=1)
    source = jnp.concatenate([tok_ref[...], cot_ref[...]], axis=0)
    send_ref[...] = dot_nn(pick, source).astype(BF16)


def fetch_kernel(gate_ref, up_ref, down_ref, pair_ref, down_out_ref):
    pair_ref[:, :LANES] = gate_ref[...]
    pair_ref[:, LANES:] = up_ref[...]
    down_out_ref[...] = down_ref[...]


def forward_kernel(
    core_ref, own_t, oth_t, own_b, oth_b, pair_ref, down_ref, near_ref, far_ref, acts_ref
):
    core = core_ref[0]
    half = own_t.shape[1]
    count = own_t.shape[0]
    chips = near_ref.shape[0]
    mine = pl.ds(pl.multiple_of(core * half, half), half)
    other = pl.ds(pl.multiple_of((1 - core) * half, half), half)
    pre = dot_nn(own_t[...], pair_ref[mine, :]) + dot_nn(oth_t[...], pair_ref[other, :])
    scaled = dot_nt(own_b[...], down_ref[:, mine]) + dot_nt(oth_b[...], down_ref[:, other])
    pre_gate = pre[:, :LANES]
    pre_up = pre[:, LANES:]
    sig = jax.nn.sigmoid(pre_gate)
    active = pre_gate * sig
    hidden = (active * pre_up).astype(BF16)
    back_gate = (scaled * pre_up * (sig * (1.0 + pre_gate * (1.0 - sig)))).astype(BF16)
    back_up = (scaled * active).astype(BF16)
    acts_ref[0] = hidden
    acts_ref[1] = back_gate
    acts_ref[2] = back_up

    mix = jnp.sum(hidden.astype(F32) * scaled, axis=1, keepdims=True)
    slot = iota((count, LANES), 0)
    spread = jnp.where(iota((count, LANES), 1) == slot % LANES, mix, 0.0)
    lines = [
        jnp.sum(jnp.where(slot // LANES == k, spread, 0.0), axis=0, keepdims=True)
        for k in range(pl.cdiv(count, LANES))
    ]
    lines += [jnp.zeros((1, LANES), F32)] * (ROWS8 - len(lines))
    table = jnp.concatenate(lines, axis=0)

    backs = jnp.concatenate([back_gate, back_up], axis=1)
    for chip in range(chips):
        for which, out in ((core, near_ref), (1 - core, far_ref)):
            cols = pl.ds(pl.multiple_of((2 * chip + which) * LANES, LANES), LANES)
            part = dot_nt(backs, pair_ref[cols, :])
            out[chip, 0:count, :] = part.astype(out.dtype)
            out[chip, count : count + ROWS8, :] = table.astype(out.dtype)


def weights_kernel(core_ref, own_t, oth_t, own_b, oth_b, acts_ref, gate_ref, up_ref, down_ref):
    core = core_ref[0]
    half = own_t.shape[1]
    mine = pl.ds(pl.multiple_of(core * half, half), half)
    other = pl.ds(pl.multiple_of((1 - core) * half, half), half)
    backs = jnp.concatenate([acts_ref[1], acts_ref[2]], axis=1)
    hidden = acts_ref[0]
    for where, rows, cots in ((mine, own_t, own_b), (other, oth_t, oth_b)):
        grads = dot_tn(rows[...], backs)
        gate_ref[where, :] = grads[:, :LANES].astype(BF16)
        up_ref[where, :] = grads[:, LANES:].astype(BF16)
        down_ref[:, where] = dot_tn(hidden, cots[...]).astype(BF16)


def gather_kernel(pieces_ref, back_ref):
    total = pieces_ref[0].astype(F32)
    for k in range(1, pieces_ref.shape[0]):
        total = total + pieces_ref[k].astype(F32)
    total = total.astype(BF16)
    rows = back_ref.shape[0]
    count = rows // ROWS8 * SLOTS
    row = iota((rows, total.shape[0]), 0)
    slot = row % ROWS8
    source = jnp.where(slot < SLOTS, row // ROWS8 * SLOTS + slot, count + slot - SLOTS)
    pick = jnp.where(iota((rows, total.shape[0]), 1) == source, 1.0, 0.0).astype(BF16)
    back_ref[...] = dot_nn(pick, total).astype(BF16)


def combine_kernel(block_ref, routes_ref, mix_ref, back_ref, token_ref, mix_out_ref):
    routes = routes_ref[...]
    mix = mix_ref[...].astype(F32)
    back = back_ref[...]
    rows = back.shape[0]
    tok = routes.shape[1]
    ranks = slots_of(routes, rows // ROWS8)
    row = iota((rows, tok), 0)
    at = [routes[k : k + 1] * ROWS8 + ranks[k] for k in range(2)]
    pick = jnp.where((row == at[0]) | (row == at[1]), 1.0, 0.0).astype(BF16)
    token_ref[...] = dot_tn(pick, back).astype(BF16)
    for k in range(2):
        slot = block_ref[0] * SLOTS + ranks[k]
        line = routes[k : k + 1] * ROWS8 + SLOTS + slot // LANES
        pick = jnp.where(row == line, 1.0, 0.0).astype(BF16)
        lines = dot_tn(back, pick)
        found = jnp.where(iota((LANES, tok), 0) == slot % LANES, lines, 0.0)
        value = jnp.sum(found, axis=0, keepdims=True) / mix[k : k + 1]
        mix_out_ref[k : k + 1, :] = value.astype(BF16)


def in_hbm(value):
    return pltpu.with_memory_space_constraint(value, pltpu.HBM)


def params():
    return pltpu.CompilerParams(vmem_limit_bytes=24 * 1024 * 1024)


def smem():
    return pl.BlockSpec(memory_space=pltpu.SMEM)


def vmem():
    return pl.BlockSpec(memory_space=pltpu.VMEM)


def call(kernel, out_shape, n_in, cost=None, name=None, scalars=1):
    outs = out_shape if isinstance(out_shape, tuple) else (out_shape,)
    specs = tuple(vmem() for _ in outs)
    return pl.pallas_call(
        kernel,
        out_shape=out_shape,
        in_specs=[smem()] * scalars + [vmem()] * n_in,
        out_specs=specs if isinstance(out_shape, tuple) else specs[0],
        cost_estimate=cost,
        compiler_params=params(),
        name=name,
    )


def on_device(tokens, cotangent, mix_weights, routes, gate_proj, up_proj, down_proj):
    experts = lax.axis_size("ep")
    chips = lax.axis_size("x")
    core = lax.axis_index("c").astype(jnp.int32).reshape(1)
    block = lax.axis_index("ep").astype(jnp.int32).reshape(1)
    tok_rows, width = tokens.shape
    count = experts * SLOTS
    half = width // 2
    tiles = half // LANES
    struct = jax.ShapeDtypeStruct
    routes_t = routes.T
    mix_t = mix_weights.T
    gate_w = gate_proj[0]
    up_w = up_proj[0]
    down_w = down_proj[0]

    send = pl.pallas_call(
        dispatch_kernel,
        out_shape=struct((2 * count, half), BF16),
        grid_spec=pltpu.PrefetchScalarGridSpec(
            num_scalar_prefetch=1,
            grid=(1,),
            in_specs=[
                pl.BlockSpec(routes_t.shape, lambda i, c: (0, 0)),
                pl.BlockSpec(mix_t.shape, lambda i, c: (0, 0)),
                pl.BlockSpec((tok_rows, half), lambda i, c: (0, c[0])),
                pl.BlockSpec((tok_rows, half), lambda i, c: (0, c[0])),
            ],
            out_specs=pl.BlockSpec((2 * count, half), lambda i, c: (0, 0)),
        ),
        compiler_params=params(),
        name="dispatch",
    )(core, *(in_hbm(a) for a in (routes_t, mix_t, tokens, cotangent)))
    send = send.reshape(experts, 2 * SLOTS * tiles, LANES)
    got = lax.all_to_all(send, "ep", 0, 0, tiled=True)
    own_t = got[:, : SLOTS * tiles].reshape(count, half)
    own_b = got[:, SLOTS * tiles :].reshape(count, half)
    oth_t = swap_cores(own_t)
    oth_b = swap_cores(own_b)
    gate_w, up_w, down_w, _ = lax.optimization_barrier((gate_w, up_w, down_w, got))
    pair_w, down_w = call(
        fetch_kernel,
        (pltpu.VMEM((width, 2 * LANES), BF16), pltpu.VMEM(down_w.shape, BF16)),
        3,
        name="fetch",
        scalars=0,
    )(*(in_hbm(w) for w in (gate_w, up_w, down_w)))

    shape = (chips, count + ROWS8, LANES)
    near, far, acts = call(
        forward_kernel,
        (struct(shape, F32), struct(shape, BF16), struct((3, count, LANES), BF16)),
        6,
        name="forward",
    )(core, own_t, oth_t, own_b, oth_b, pair_w, down_w)
    theirs = swap_cores(far)
    pair = (near + theirs.astype(F32)).astype(BF16)
    pieces = lax.all_to_all(pair, "x", 0, 0, tiled=True)
    back = pl.pallas_call(
        gather_kernel,
        out_shape=struct((experts * ROWS8, LANES), BF16),
        compiler_params=params(),
        name="gather",
    )(pieces)
    acts, back = lax.optimization_barrier((acts, back))
    gate_grad, up_grad, down_grad = call(
        weights_kernel,
        (struct((width, LANES), BF16), struct((width, LANES), BF16), struct((LANES, width), BF16)),
        5,
        cost=pl.CostEstimate(
            flops=6 * count * width * LANES, bytes_accessed=6 * width * LANES, transcendentals=0
        ),
        name="weights",
    )(core, own_t, oth_t, own_b, oth_b, acts)
    back = lax.all_to_all(back.reshape(experts, ROWS8, LANES), "ep", 0, 0, tiled=True)
    token_grad, mix_grad = call(
        combine_kernel,
        (struct((tok_rows, LANES), BF16), struct(mix_t.shape, BF16)),
        3,
        name="combine",
    )(block, routes_t, mix_t, back.reshape(experts * ROWS8, LANES))
    return (token_grad, mix_grad.T, gate_grad[None], up_grad[None], down_grad[None])


def solution(mesh):
    ep = mesh.shape["ep"]
    split = Mesh(mesh.devices.reshape(ep, mesh.shape["tp"] // 2, 2), ("ep", "x", "c"))
    tp = ("x", "c")
    in_specs = (
        P("ep", None),
        P("ep", None),
        P("ep", None),
        P("ep", None),
        P("ep", None, tp),
        P("ep", None, tp),
        P("ep", tp, None),
    )
    out_specs = (
        P("ep", tp),
        P("ep", None),
        P("ep", None, tp),
        P("ep", None, tp),
        P("ep", tp, None),
    )
    return jax.shard_map(
        on_device, mesh=split, in_specs=in_specs, out_specs=out_specs, check_vma=False
    )
```

time: 133 us -> 124 us (0.932)
  blocking collectives: 57.1 us -> 84.4 us
  waiting for transfers between devices: 29 us -> 11.8 us
  matrix products: 11.6 us -> 0 us
  Pallas kernels: 0 us -> 9.07 us
  local copies, waits for them, and re-layouts: 8.73 us -> 1.29 us
  starting transfers between devices: 22.6 us -> 15.8 us
  other arithmetic: 2.58 us -> 0.16 us
    all_to_all x0 -> x1, blocking collectives: none -> 27.3 us  [on_device(): pieces = lax.all_to_all(pair, 'x', 0, 0, tiled=True)]
    all_to_all x2 -> x1, waiting for transfers between devices: 27.4 us -> 9.34 us  [on_device(): lax.all_to_all(back.reshape(experts, ROWS8, LANES), 'ep', 0, 0, tiled=True)]
    dot_general x13 -> x0, matrix products: 11.6 us -> none  [the longest x1 2.37 us: on_device(): lax.dot_general(hidden, backs, (((0,), (0,)), ((), ())), preferred_elemen...]
    pallas_call x0 -> x6, Pallas kernels: none -> 9.07 us  [the longest x1 2.17 us: on_device(): call(weights_kernel, (struct((width, LANES), BF16), struct((width, LANES)...]
    all_to_all x2 -> x1, starting transfers between devices: 13.2 us -> 6.72 us  [on_device(): lax.all_to_all(back.reshape(experts, ROWS8, LANES), 'ep', 0, 0, tiled=True)]
    dynamic_slice x1 -> x0, local copies, waits for them, and re-layouts: 2.71 us -> none  [for_core(): piece = lax.dynamic_index_in_dim(part, which, 2, keepdims=False)]
    unnamed x26 -> x4, local copies, waits for them, and re-layouts: 2.08 us -> 0.01 us
  transfers between devices with their start and end apart: 5 -> 4, of which waited for: 3 -> 3; matrix products, arithmetic and copies ran while one was open for 5% -> 0% of each run, Pallas kernels for 0% -> 3%
where the time goes in v2:
time: 124 us; the launch traced here: 123 us
  blocking collectives  84.4 us (68%)
  starting transfers between devices  15.8 us (13%)
  waiting for transfers between devices  11.8 us (10%)
  Pallas kernels  9.07 us (7%)
  local copies, waits for them, and re-layouts  1.29 us (1%)
    all_to_all x1, blocking collectives, on_device(): got = lax.all_to_all(send, 'ep', 0, 0, tiled=True)  57 us
    all_to_all x1, blocking collectives, on_device(): pieces = lax.all_to_all(pair, 'x', 0, 0, tiled=True)  27.3 us
    all_to_all x1, waiting for transfers between devices, on_device(): lax.all_to_all(back.reshape(experts, ROWS8, LANES), 'ep', 0, 0, tiled=True)  9.34 us
    ppermute x3, starting transfers between devices, swap_cores(): return lax.ppermute(value, 'c', [(0, 1), (1, 0)])  9.1 us
    all_to_all x1, starting transfers between devices, on_device(): lax.all_to_all(back.reshape(experts, ROWS8, LANES), 'ep', 0, 0, tiled=True)  6.72 us
  transfers between devices with their start and end apart: 4, of which 3 were waited for; matrix products, arithmetic and copies ran while one was open for 0% of the time, Pallas kernels for 3%

profile of v2, /device:TPU:1, one launch (start us, length us, event | category | flops | bytes accessed | tf_op | source)
XLA Modules:
  0.0 123.2 jit_solution(5600801024256314372)
XLA Ops:
  0.6 1.7 %dispatch.1 = bf16[640,1024]{1,0:T(8,128)(2,1)S(1)} custom-call(s32[1]{0:T(128)} %bitcast.3.core_ref, s32[2,128]{1,0:T(2,128)} %bitcast.14, bf16[2,128]{1,0:T(2,128)(2,1)} %bitcast.16, bf16[128,2048]{1,0:T(8,128)(2,1)} %tok_ref.1, bf16[128,2048]{1,0:T(8,128)(2,1)} %cot_ref.1), custom_call_target="tpu_custom_call" | custom-call | tf_op jit(solution)/shard_map/dispatch/pallas_call | solution.py:210
  2.3 0.6 reshape.33
  3.0 57.0 %all_to_all.15 = bf16[64,80,128]{2,1,0:T(8,128)(2,1)S(1)} all-to-all(bf16[64,80,128]{2,1,0:T(8,128)(2,1)S(1)} %reshape.33), channel_id=1, replica_groups=mesh['ep'=64,'x'=8,'c'=2] {'ep'}, dimensions={0} | all-to-all | bytes 2621440 | tf_op jit(solution)/shard_map/all_to_all | solution.py:228
  60.0 0.1 fusion
  60.1 0.3 reshape.35.own_b
  60.4 0.3 reshape.34.own_t
  60.7 5.1 %collective-permute-start = (bf16[320,1024]{1,0:T(8,128)(2,1)S(1)}, bf16[320,1024]{1,0:T(8,128)(2,1)S(1)}, u32[]{:S(2)}, u32[]{:S(2)}) collective-permute-start(bf16[320,1024]{1,0:T(8,128)(2,1)S(1)} %reshape.34.own_t), channel_id=1, source_target_pairs={{0,1},{1,0},{2,3},{3,2},{4,5},{5,4},{6,7},{7,6},{8,9},{9,8},{10,11... | collective-permute-start | bytes 1966088 | tf_op jit(solution)/shard_map/ppermute | solution.py:33
  65.8 1.9 %collective-permute-start.1 = (bf16[320,1024]{1,0:T(8,128)(2,1)S(1)}, bf16[320,1024]{1,0:T(8,128)(2,1)S(1)}, u32[]{:S(2)}, u32[]{:S(2)}) collective-permute-start(bf16[320,1024]{1,0:T(8,128)(2,1)S(1)} %reshape.35.own_b), channel_id=1, source_target_pairs={{0,1},{1,0},{2,3},{3,2},{4,5},{5,4},{6,7},{7,6},{8,9},{9,8},{10,11... | collective-permute-start | bytes 1966088 | tf_op jit(solution)/shard_map/ppermute | solution.py:33
  67.8 1.6 %fetch.1 = (bf16[2048,256]{1,0:T(8,128)(2,1)S(1)}, bf16[128,2048]{1,0:T(8,128)(2,1)S(1)}) custom-call(bf16[2048,128]{1,0:T(8,128)(2,1)} %bitcast.18, bf16[2048,128]{1,0:T(8,128)(2,1)} %bitcast.19, bf16[128,2048]{1,0:T(8,128)(2,1)} %bitcast.20), custom_call_target="tpu_custom_call" | custom-call | tf_op jit(solution)/shard_map/fetch/pallas_call | solution.py:234
  69.3 0.0 collective-permute-done.oth_t
  69.3 0.5 collective-permute-done.1.oth_b
  69.8 1.6 %forward.1 = (f32[8,328,128]{2,1,0:T(8,128)S(1)}, bf16[8,328,128]{2,1,0:T(8,128)(2,1)S(1)}, bf16[3,320,128]{2,1,0:T(8,128)(2,1)S(1)}) custom-call(s32[1]{0:T(128)} %bitcast.3.core_ref, bf16[320,1024]{1,0:T(8,128)(2,1)S(1)} %reshape.34.own_t, bf16[320,1024]{1,0:T(8,128)(2,1)S(1)} %collective-permute-done.oth_t, bf16[320,1024]{1,0:T(8,128)(2,1)S(1)} %reshape.35.own_b, ...), custom_call_target="tpu_custom_call" | custom-call | tf_op jit(solution)/shard_map/forward/pallas_call | solution.py:243
  71.4 2.0 %collective-permute-start.2 = (bf16[8,328,128]{2,1,0:T(8,128)(2,1)S(1)}, bf16[8,328,128]{2,1,0:T(8,128)(2,1)S(1)}, u32[]{:S(2)}, u32[]{:S(2)}) collective-permute-start(bf16[8,328,128]{2,1,0:T(8,128)(2,1)S(1)} %get-tuple-element.27), channel_id=1, source_target_pairs={{0,1},{1,0},{2,3},{3,2},{4,5},{5,4},{6,7},{7,6},{8,9},{9,8},{10,11... | collective-permute-start | bytes 2015240 | tf_op jit(solution)/shard_map/ppermute | solution.py:33
  73.5 2.0 %collective-permute-done.2 = bf16[8,328,128]{2,1,0:T(8,128)(2,1)S(1)} collective-permute-done((bf16[8,328,128]{2,1,0:T(8,128)(2,1)S(1)}, bf16[8,328,128]{2,1,0:T(8,128)(2,1)S(1)}, u32[]{:S(2)}, u32[]{:S(2)}) %collective-permute-start.2) | collective-permute-done | bytes 671776 | tf_op jit(solution)/shard_map/ppermute | solution.py:33
  75.5 0.2 add_convert_fusion
  75.6 27.3 %all_to_all.16.pieces_ref = bf16[8,328,128]{2,1,0:T(8,128)(2,1)S(1)} all-to-all(bf16[8,328,128]{2,1,0:T(8,128)(2,1)S(1)} %add_convert_fusion), channel_id=1, replica_groups=mesh['ep'=64,'x'=8,'c'=2] {'x'}, dimensions={0} | all-to-all | bytes 1343488 | tf_op jit(solution)/shard_map/all_to_all | solution.py:251
  102.9 1.0 gather.1
  103.9 6.7 %all-to-all-start.2 = ((bf16[64,8,128]{2,1,0:T(8,128)(2,1)}), bf16[64,8,128]{2,1,0:T(8,128)(2,1)S(1)}, u32[]{:S(2)}, u32[]{:S(2)}) async-start(bf16[64,8,128]{2,1,0:T(8,128)(2,1)} %bitcast.7), calls=%async_computation.2 | async-start | bytes 262144 | tf_op jit(solution)/shard_map/all_to_all | solution.py:268
  110.6 0.0 copy-start
  110.7 0.0 copy-start.1
  110.7 2.2 %weights.1 = (bf16[2048,128]{1,0:T(8,128)(2,1)}, bf16[2048,128]{1,0:T(8,128)(2,1)}, bf16[128,2048]{1,0:T(8,128)(2,1)}) custom-call(s32[1]{0:T(128)} %bitcast.3.core_ref, bf16[320,1024]{1,0:T(8,128)(2,1)S(1)} %reshape.34.own_t, bf16[320,1024]{1,0:T(8,128)(2,1)S(1)} %collective-permute-done.oth_t, bf16[320,1024]{1,0:T(8,128)(2,1)S(1)} %reshape.35.own_b, ...), custom_call_target="tpu_custom_call" | custom-call | flops 503316480 | bytes 1572864 | tf_op jit(solution)/shard_map/weights/pallas_call | solution.py:259
  112.8 9.3 %all-to-all-done.2 = bf16[64,8,128]{2,1,0:T(8,128)(2,1)S(1)} async-done(((bf16[64,8,128]{2,1,0:T(8,128)(2,1)}), bf16[64,8,128]{2,1,0:T(8,128)(2,1)S(1)}, u32[]{:S(2)}, u32[]{:S(2)}) %all-to-all-start.2) | async-done | bytes 131104 | tf_op jit(solution)/shard_map/all_to_all | solution.py:268
  122.2 0.0 copy-done
  122.2 0.0 copy-done.1
  122.2 1.0 combine.1
Async XLA Ops:
  60.7 8.6 %collective-permute-start = (bf16[320,1024]{1,0:T(8,128)(2,1)S(1)}, bf16[320,1024]{1,0:T(8,128)(2,1)S(1)}, u32[]{:S(2)}, u32[]{:S(2)}) collective-permute-start(bf16[320,1024]{1,0:T(8,128)(2,1)S(1)} %reshape.34.own_t), channel_id=1, source_target_pairs={{0,1},{1,0},{2,3},{3,2},{4,5},{5,4},{6,7},{7,6},{8,9},{9,8},{10,11... | collective-permute-start | bytes 1966088 | tf_op jit(solution)/shard_map/ppermute | solution.py:33
  65.8 4.0 %collective-permute-start.1 = (bf16[320,1024]{1,0:T(8,128)(2,1)S(1)}, bf16[320,1024]{1,0:T(8,128)(2,1)S(1)}, u32[]{:S(2)}, u32[]{:S(2)}) collective-permute-start(bf16[320,1024]{1,0:T(8,128)(2,1)S(1)} %reshape.35.own_b), channel_id=1, source_target_pairs={{0,1},{1,0},{2,3},{3,2},{4,5},{5,4},{6,7},{7,6},{8,9},{9,8},{10,11... | collective-permute-start | bytes 1966088 | tf_op jit(solution)/shard_map/ppermute | solution.py:33
  71.4 4.0 %collective-permute-start.2 = (bf16[8,328,128]{2,1,0:T(8,128)(2,1)S(1)}, bf16[8,328,128]{2,1,0:T(8,128)(2,1)S(1)}, u32[]{:S(2)}, u32[]{:S(2)}) collective-permute-start(bf16[8,328,128]{2,1,0:T(8,128)(2,1)S(1)} %get-tuple-element.27), channel_id=1, source_target_pairs={{0,1},{1,0},{2,3},{3,2},{4,5},{5,4},{6,7},{7,6},{8,9},{9,8},{10,11... | collective-permute-start | bytes 2015240 | tf_op jit(solution)/shard_map/ppermute | solution.py:33
  103.9 18.3 %all-to-all-start.2 = ((bf16[64,8,128]{2,1,0:T(8,128)(2,1)}), bf16[64,8,128]{2,1,0:T(8,128)(2,1)S(1)}, u32[]{:S(2)}, u32[]{:S(2)}) async-start(bf16[64,8,128]{2,1,0:T(8,128)(2,1)} %bitcast.7), calls=%async_computation.2 | async-start | bytes 262144 | tf_op jit(solution)/shard_map/all_to_all | solution.py:268
  110.6 11.5 %copy-start = (s32[128,2]{0,1:T(2,128)S(1)}, s32[128,2]{0,1:T(2,128)}, u32[]{:S(2)}) copy-start(s32[128,2]{0,1:T(2,128)} %param.10) | copy-start | bytes 3076
  110.7 11.5 %copy-start.1 = (bf16[128,2]{0,1:T(2,128)(2,1)S(1)}, bf16[128,2]{0,1:T(2,128)(2,1)}, u32[]{:S(2)}) copy-start(bf16[128,2]{0,1:T(2,128)(2,1)} %param.9) | copy-start | bytes 1540

commit v3 on v2

v3 whole, which is shorter than its diff:
```python
import functools

import jax
import jax.numpy as jnp
from jax import lax
from jax.experimental import pallas as pl
from jax.experimental.pallas import tpu as pltpu
from jax.sharding import Mesh
from jax.sharding import PartitionSpec as P


SLOTS = 5
PART = 3
LANES = 128
ROWS8 = 8
F32 = jnp.float32
BF16 = jnp.bfloat16


def iota(shape, dim):
    return lax.broadcasted_iota(jnp.int32, shape, dim)


def dot_nn(a, b):
    return lax.dot_general(a, b, (((1,), (0,)), ((), ())), preferred_element_type=F32)


def dot_nt(a, b):
    return lax.dot_general(a, b, (((1,), (1,)), ((), ())), preferred_element_type=F32)


def dot_tn(a, b):
    return lax.dot_general(a, b, (((0,), (0,)), ((), ())), preferred_element_type=F32)


def swap_cores(value):
    return lax.ppermute(value, "c", [(0, 1), (1, 0)])


def slots_of(routes, experts):
    tok = routes.shape[1]
    ids = iota((experts, tok), 0)
    named = [ids == routes[k : k + 1] for k in range(2)]
    both = jnp.where(named[0] | named[1], 1.0, 0.0).astype(BF16)
    earlier = jnp.where(iota((tok, tok), 0) < iota((tok, tok), 1), 1.0, 0.0).astype(BF16)
    before = dot_nn(both, earlier)
    return [
        jnp.sum(jnp.where(hit, before, 0.0), axis=0, keepdims=True).astype(jnp.int32)
        for hit in named
    ]


def dispatch_kernel(place_ref, routes_ref, mix_ref, tok_ref, cot_ref, send_ref):
    routes = routes_ref[...]
    mix = mix_ref[...].astype(F32)
    experts = send_ref.shape[0]
    count = experts * 2 * PART
    tok = routes.shape[1]
    ranks = slots_of(routes, experts)
    first = place_ref[1] * PART
    at = []
    for k in range(2):
        slot = ranks[k] - first
        kept = (slot >= 0) & (slot < PART)
        at.append(jnp.where(kept, routes[k : k + 1] * (2 * PART) + slot, -count))
    row = iota((count, tok), 0)
    place = jnp.where((row == at[0]) | (row == at[1]), 1.0, 0.0)
    scale = jnp.where(
        row == at[0] + PART, mix[0:1], jnp.where(row == at[1] + PART, mix[1:2], 0.0)
    )
    pick = jnp.concatenate([place.astype(BF16), scale.astype(BF16)], axis=1)
    source = jnp.concatenate([tok_ref[...], cot_ref[...]], axis=0)
    send_ref[...] = dot_nn(pick, source).astype(BF16).reshape(send_ref.shape)


def unpacked(wire_ref):
    experts, lines, _ = wire_ref.shape
    cut = lines // 2
    shape = (experts * PART, cut // PART * LANES)
    return wire_ref[:, :cut, :].reshape(shape), wire_ref[:, cut:, :].reshape(shape)


def unpack_kernel(wire_ref, mark_ref, gate_hbm, up_hbm, down_hbm, *refs):
    del mark_ref
    rows_ref, cots_ref, gate_ref, up_ref, down_ref, sems = refs
    pairs = ((gate_hbm, gate_ref), (up_hbm, up_ref), (down_hbm, down_ref))
    copies = [pltpu.make_async_copy(a, b, sems.at[k]) for k, (a, b) in enumerate(pairs)]
    for copy in copies:
        copy.start()
    rows_ref[...], cots_ref[...] = unpacked(wire_ref)
    for copy in copies:
        copy.wait()


def mark_kernel(core_ref, out_ref):
    out_ref[...] = jnp.zeros(out_ref.shape, F32) + core_ref[0].astype(F32)


def forward_kernel(place_ref, own_t, own_b, wire_ref, *refs):
    weights = (refs[0:3], refs[3:6])
    near_ref, far_ref, acts_ref, oth_t, oth_b = refs[6:]
    oth_t[...], oth_b[...] = unpacked(wire_ref)
    core = place_ref[0]
    count, half = own_t.shape
    chips = near_ref.shape[0]
    mine = pl.ds(pl.multiple_of(core * half, half), half)
    other = pl.ds(pl.multiple_of((1 - core) * half, half), half)

    backs = []
    mix = jnp.zeros((count, 1), F32)
    for k, (gate_ref, up_ref, down_ref) in enumerate(weights):
        pre = sum(
            dot_nn(rows[...], jnp.concatenate([gate_ref[where, :], up_ref[where, :]], axis=1))
            for rows, where in ((own_t, mine), (oth_t, other))
        )
        scaled = dot_nt(own_b[...], down_ref[:, mine]) + dot_nt(oth_b[...], down_ref[:, other])
        pre_gate = pre[:, :LANES]
        pre_up = pre[:, LANES:]
        sig = jax.nn.sigmoid(pre_gate)
        active = pre_gate * sig
        hidden = (active * pre_up).astype(BF16)
        back_gate = (scaled * pre_up * (sig * (1.0 + pre_gate * (1.0 - sig)))).astype(BF16)
        back_up = (scaled * active).astype(BF16)
        acts_ref[k, 0] = hidden
        acts_ref[k, 1] = back_gate
        acts_ref[k, 2] = back_up
        backs += [back_gate, back_up]
        mix = mix + jnp.sum(hidden.astype(F32) * scaled, axis=1, keepdims=True)

    row = iota((count, LANES), 0)
    source = (row * 171) >> 9
    slot = source * SLOTS + place_ref[1] * PART + (row - source * PART)
    spread = jnp.where(iota((count, LANES), 1) == slot % LANES, mix, 0.0)
    lines = [
        jnp.sum(jnp.where(slot // LANES == k, spread, 0.0), axis=0, keepdims=True)
        for k in range(ROWS8 - SLOTS)
    ]
    lines += [jnp.zeros((1, LANES), F32)] * SLOTS
    table = jnp.concatenate(lines, axis=0)

    backs = jnp.concatenate(backs, axis=1)
    for chip in range(chips):
        for which, out in ((core, near_ref), (1 - core, far_ref)):
            cols = pl.ds(pl.multiple_of((2 * chip + which) * LANES, LANES), LANES)
            rhs = jnp.concatenate([w[cols, :] for g in weights for w in g[:2]], axis=1)
            out[chip, 0:count, :] = dot_nt(backs, rhs).astype(out.dtype)
            out[chip, count : count + ROWS8, :] = table.astype(out.dtype)


def weights_kernel(which, place_ref, own_t, oth_t, own_b, oth_b, acts_ref, *outs):
    gate_ref, up_ref, down_ref = outs
    core = place_ref[0]
    half = own_t.shape[1]
    mine = pl.ds(pl.multiple_of(core * half, half), half)
    other = pl.ds(pl.multiple_of((1 - core) * half, half), half)
    backs = jnp.concatenate([acts_ref[which, 1], acts_ref[which, 2]], axis=1)
    hidden = acts_ref[which, 0]
    for where, rows, cots in ((mine, own_t, own_b), (other, oth_t, oth_b)):
        grads = dot_tn(rows[...], backs)
        gate_ref[where, :] = grads[:, :LANES].astype(gate_ref.dtype)
        up_ref[where, :] = grads[:, LANES:].astype(up_ref.dtype)
        down_ref[:, where] = dot_tn(hidden, cots[...]).astype(down_ref.dtype)


def add_kernel(*refs):
    for own, got, out in zip(refs[0:3], refs[3:6], refs[6:9]):
        out[...] = (own[...] + got[...].astype(F32)).astype(out.dtype)


def gather_kernel(pieces_ref, back_ref):
    chips, lines, _ = pieces_ref.shape
    count = lines - ROWS8
    sums = []
    for parity in range(2):
        total = pieces_ref[parity].astype(F32)
        for k in range(parity + 2, chips, 2):
            total = total + pieces_ref[k].astype(F32)
        sums.append(total)
    table = sums[0][count:] + sums[1][count:]
    total = jnp.concatenate([sums[0][:count], sums[1][:count], table], axis=0).astype(BF16)
    rows = back_ref.shape[0]
    row = iota((rows, total.shape[0]), 0)
    source = (row >> 3) * PART
    slot = row & 7
    source = jnp.where(
        slot < PART,
        source + slot,
        jnp.where(slot < SLOTS, count + source + slot - PART, 2 * count + slot - SLOTS),
    )
    pick = jnp.where(iota((rows, total.shape[0]), 1) == source, 1.0, 0.0).astype(BF16)
    back_ref[...] = dot_nn(pick, total).astype(BF16)


def combine_kernel(block_ref, routes_ref, mix_ref, back_ref, token_ref, mix_out_ref):
    routes = routes_ref[...]
    mix = mix_ref[...].astype(F32)
    back = back_ref[...]
    rows = back.shape[0]
    tok = routes.shape[1]
    ranks = slots_of(routes, rows // ROWS8)
    row = iota((rows, tok), 0)
    at = [routes[k : k + 1] * ROWS8 + ranks[k] for k in range(2)]
    pick = jnp.where((row == at[0]) | (row == at[1]), 1.0, 0.0).astype(BF16)
    token_ref[...] = dot_tn(pick, back).astype(BF16)
    for k in range(2):
        slot = block_ref[0] * SLOTS + ranks[k]
        line = routes[k : k + 1] * ROWS8 + SLOTS + slot // LANES
        pick = jnp.where(row == line, 1.0, 0.0).astype(BF16)
        lines = dot_tn(back, pick)
        found = jnp.where(iota((LANES, tok), 0) == slot % LANES, lines, 0.0)
        value = jnp.sum(found, axis=0, keepdims=True) / mix[k : k + 1]
        mix_out_ref[k : k + 1, :] = value.astype(BF16)


def in_hbm(value):
    return pltpu.with_memory_space_constraint(value, pltpu.HBM)


def params():
    return pltpu.CompilerParams(vmem_limit_bytes=24 * 1024 * 1024)


def smem():
    return pl.BlockSpec(memory_space=pltpu.SMEM)


def vmem():
    return pl.BlockSpec(memory_space=pltpu.VMEM)


def call(kernel, out_shape, n_in, cost=None, scalars=1, n_hbm=0, scratch=()):
    outs = out_shape if isinstance(out_shape, tuple) else (out_shape,)
    specs = tuple(vmem() for _ in outs)
    return pl.pallas_call(
        kernel,
        out_shape=out_shape,
        in_specs=[smem()] * scalars + [vmem()] * n_in + [pl.BlockSpec(memory_space=pl.ANY)] * n_hbm,
        scratch_shapes=scratch,
        out_specs=specs if isinstance(out_shape, tuple) else specs[0],
        cost_estimate=cost,
        compiler_params=params(),
    )


def on_device(tokens, cotangent, mix_weights, routes, gate_proj, up_proj, down_proj):
    experts = lax.axis_size("ep")
    chips = lax.axis_size("x")
    place = jnp.stack([lax.axis_index("c"), lax.axis_index("x") & 1]).astype(jnp.int32)
    block = lax.axis_index("ep").astype(jnp.int32).reshape(1)
    tok_rows, width = tokens.shape
    count = experts * PART
    half = width // 2
    wire = (experts, 2 * PART * half // LANES, LANES)
    struct = jax.ShapeDtypeStruct
    routes_t = routes.T
    mix_t = mix_weights.T
    own_w = (gate_proj[0], up_proj[0], down_proj[0])

    lend = []
    for k in range(chips):
        lend += [(2 * k, 2 * ((k - 1) % chips)), (2 * k + 1, 2 * ((k + 1) % chips) + 1)]
    give_back = [(b, a) for a, b in lend]

    send = pl.pallas_call(
        dispatch_kernel,
        out_shape=struct(wire, BF16),
        grid_spec=pltpu.PrefetchScalarGridSpec(
            num_scalar_prefetch=1,
            grid=(1,),
            in_specs=[
                pl.BlockSpec(routes_t.shape, lambda i, c: (0, 0)),
                pl.BlockSpec(mix_t.shape, lambda i, c: (0, 0)),
                pl.BlockSpec((tok_rows, half), lambda i, c: (0, c[0])),
                pl.BlockSpec((tok_rows, half), lambda i, c: (0, c[0])),
            ],
            out_specs=pl.BlockSpec(wire, lambda i, c: (0, 0, 0)),
        ),
        compiler_params=params(),
        name="dispatch",
    )(place, *(in_hbm(a) for a in (routes_t, mix_t, tokens, cotangent)))
    got = lax.all_to_all(send, "ep", 0, 0, tiled=True)
    lent_w = tuple(lax.ppermute(w, ("x", "c"), lend) for w in own_w)
    mark = call(mark_kernel, struct((8, LANES), F32), 0)(place)
    theirs = swap_cores(got)
    rows = struct((count, half), BF16)
    in_vmem = [pltpu.VMEM(w.shape, BF16) for w in own_w]
    copies = pltpu.SemaphoreType.DMA((3,))
    own_t, own_b, *held_w = call(
        unpack_kernel, (rows, rows, *in_vmem), 2, scalars=0, n_hbm=3, scratch=(copies,)
    )(got, mark, *(in_hbm(w) for w in own_w))

    shape = (chips, count + ROWS8, LANES)
    near, far, acts, oth_t, oth_b = call(
        forward_kernel,
        (struct(shape, F32), struct(shape, BF16), struct((2, 3, count, LANES), BF16), rows, rows),
        9,
    )(place, own_t, own_b, theirs, *held_w, *lent_w)
    theirs = swap_cores(far)
    pair = (near + theirs.astype(F32)).astype(BF16)
    pieces = lax.all_to_all(pair, "x", 0, 0, tiled=True)

    shapes = ((width, LANES), (width, LANES), (LANES, width))
    cost = pl.CostEstimate(
        flops=6 * count * width * LANES, bytes_accessed=6 * width * LANES, transcendentals=0
    )
    grads = [
        call(
            functools.partial(weights_kernel, k),
            tuple(pltpu.VMEM(s, F32 if k == 0 else BF16) for s in shapes),
            5,
            cost=cost,
        )(place, own_t, oth_t, own_b, oth_b, acts)
        for k in (1, 0)
    ]
    given = tuple(lax.ppermute(g, ("x", "c"), give_back) for g in grads[0])

    back = pl.pallas_call(
        gather_kernel,
        out_shape=struct((experts * ROWS8, LANES), BF16),
        compiler_params=params(),
        name="gather",
    )(pieces)
    back = lax.all_to_all(back.reshape(experts, ROWS8, LANES), "ep", 0, 0, tiled=True)
    token_grad, mix_grad = call(
        combine_kernel, (struct((tok_rows, LANES), BF16), struct(mix_t.shape, BF16)), 3
    )(block, routes_t, mix_t, back.reshape(experts * ROWS8, LANES))
    gate_grad, up_grad, down_grad = call(
        add_kernel, tuple(struct(s, BF16) for s in shapes), 6, scalars=0
    )(*grads[1], *given)
    return (token_grad, mix_grad.T, gate_grad[None], up_grad[None], down_grad[None])


def solution(mesh):
    ep = mesh.shape["ep"]
    split = Mesh(mesh.devices.reshape(ep, mesh.shape["tp"] // 2, 2), ("ep", "x", "c"))
    tp = ("x", "c")
    in_specs = (
        P("ep", None),
        P("ep", None),
        P("ep", None),
        P("ep", None),
        P("ep", None, tp),
        P("ep", None, tp),
        P("ep", tp, None),
    )
    out_specs = (
        P("ep", tp),
        P("ep", None),
        P("ep", None, tp),
        P("ep", None, tp),
        P("ep", tp, None),
    )
    return jax.shard_map(
        on_device, mesh=split, in_specs=in_specs, out_specs=out_specs, check_vma=False
    )
```

time: 124 us -> 127 us (1.024)
  blocking collectives: 84.4 us -> 45.8 us
  starting transfers between devices: 15.8 us -> 40 us
  waiting for transfers between devices: 11.8 us -> 22.6 us
  Pallas kernels: 9.07 us -> 15.4 us
    all_to_all x1 -> x0, blocking collectives: 27.3 us -> none  [on_device(): pieces = lax.all_to_all(pair, 'x', 0, 0, tiled=True)]
    ppermute x0 -> x6, starting transfers between devices: none -> 20.1 us  [the longest x3 10.7 us: on_device(): given = tuple((lax.ppermute(g, ('x', 'c'), give_back) for g in grads[0]))]
    ppermute x0 -> x6, waiting for transfers between devices: none -> 15.5 us  [the longest x3 11 us: on_device(): lent_w = tuple((lax.ppermute(w, ('x', 'c'), lend) for w in own_w))]
    all_to_all x1, blocking collectives: 57 us -> 45.8 us  [on_device(): got = lax.all_to_all(send, 'ep', 0, 0, tiled=True)]
    all_to_all x0 -> x1, starting transfers between devices: none -> 6.46 us  [on_device(): pieces = lax.all_to_all(pair, 'x', 0, 0, tiled=True)]
    pallas_call x4 -> x7, Pallas kernels: 7.05 us -> 13.4 us  [the longest x2 3.53 us: on_device(): call(functools.partial(weights_kernel, k), tuple((pltpu.VMEM(s, F32 if k...]
    all_to_all x1, waiting for transfers between devices: 9.34 us -> 3.28 us  [on_device(): lax.all_to_all(back.reshape(experts, ROWS8, LANES), 'ep', 0, 0, tiled=True)]
    all_to_all x0 -> x1, waiting for transfers between devices: none -> 2.42 us  [on_device(): pieces = lax.all_to_all(pair, 'x', 0, 0, tiled=True)]
  transfers between devices with their start and end apart: 4 -> 10, of which waited for: 3 -> 6; matrix products, arithmetic and copies ran while one was open for 0% -> 0% of each run, Pallas kernels for 3% -> 7%
where the time goes in v3:
time: 127 us; the launch traced here: 126 us
  blocking collectives  45.8 us (36%)
  starting transfers between devices  40 us (31%)
  waiting for transfers between devices  22.6 us (18%)
  Pallas kernels  15.4 us (12%)
    all_to_all x1, blocking collectives, on_device(): got = lax.all_to_all(send, 'ep', 0, 0, tiled=True)  45.8 us
    ppermute x3, waiting for transfers between devices, on_device(): lent_w = tuple((lax.ppermute(w, ('x', 'c'), lend) for w in own_w))  11 us
    ppermute x3, starting transfers between devices, on_device(): given = tuple((lax.ppermute(g, ('x', 'c'), give_back) for g in grads[0]))  10.7 us
    ppermute x3, starting transfers between devices, on_device(): lent_w = tuple((lax.ppermute(w, ('x', 'c'), lend) for w in own_w))  9.37 us
    ppermute x2, starting transfers between devices, swap_cores(): return lax.ppermute(value, 'c', [(0, 1), (1, 0)])  7.08 us
    all_to_all x1, starting transfers between devices, on_device(): pieces = lax.all_to_all(pair, 'x', 0, 0, tiled=True)  6.46 us
    all_to_all x1, starting transfers between devices, on_device(): lax.all_to_all(back.reshape(experts, ROWS8, LANES), 'ep', 0, 0, tiled=True)  6.34 us
    ppermute x3, waiting for transfers between devices, on_device(): given = tuple((lax.ppermute(g, ('x', 'c'), give_back) for g in grads[0]))  4.55 us
  transfers between devices with their start and end apart: 10, of which 6 were waited for; matrix products, arithmetic and copies ran while one was open for 0% of the time, Pallas kernels for 7%

profile of v3, /device:TPU:1, one launch (start us, length us, event | category | flops | bytes accessed | tf_op | source)
XLA Modules:
  0.0 126.3 jit_solution(5147202461725919258)
XLA Ops:
  0.6 0.1 pad_add_fusion.place_ref.core_ref
  0.7 2.4 %dispatch.1 = bf16[64,48,128]{2,1,0:T(8,128)(2,1)S(1)} custom-call(s32[2]{0:T(128)S(1)} %pad_add_fusion.place_ref.core_ref, s32[2,128]{1,0:T(2,128)} %bitcast.15, bf16[2,128]{1,0:T(2,128)(2,1)} %bitcast.17, bf16[128,2048]{1,0:T(8,128)(2,1)} %tok_ref.1, bf16[128,2048]{1,0:T(8,128)(2,1)} %cot_ref.1), custom_call_target="tpu_custom_call" | custom-call | tf_op jit(solution)/shard_map/dispatch/pallas_call | solution.py:264
  3.1 0.0 copy-start.2
  3.1 0.0 copy-start.3
  3.1 0.0 copy-start.4
  3.1 45.8 %all_to_all.15.wire_ref = bf16[64,48,128]{2,1,0:T(8,128)(2,1)S(1)} all-to-all(bf16[64,48,128]{2,1,0:T(8,128)(2,1)S(1)} %dispatch.1), channel_id=1, replica_groups=mesh['ep'=64,'x'=8,'c'=2] {'ep'}, dimensions={0} | all-to-all | bytes 1572864 | tf_op jit(solution)/shard_map/all_to_all | solution.py:281
  49.0 4.8 %collective-permute-start = (bf16[64,48,128]{2,1,0:T(8,128)(2,1)S(1)}, bf16[64,48,128]{2,1,0:T(8,128)(2,1)S(1)}, u32[]{:S(2)}, u32[]{:S(2)}) collective-permute-start(bf16[64,48,128]{2,1,0:T(8,128)(2,1)S(1)} %all_to_all.15.wire_ref), channel_id=1, source_target_pairs={{0,1},{1,0},{2,3},{3,2},{4,5},{5,4},{6,7},{7,6},{8,9},{9,8},{10,11... | collective-permute-start | bytes 2359304 | tf_op jit(solution)/shard_map/ppermute | solution.py:37
  53.8 0.0 copy-done.2
  53.8 3.1 %collective-permute-start.1 = (bf16[2048,128]{1,0:T(8,128)(2,1)S(1)}, bf16[2048,128]{1,0:T(8,128)(2,1)S(1)}, u32[]{:S(2)}, u32[]{:S(2)}) collective-permute-start(bf16[2048,128]{1,0:T(8,128)(2,1)S(1)} %bitcast.20), channel_id=1, source_target_pairs={{0,14},{1,3},{2,0},{3,5},{4,2},{5,7},{6,4},{7,9},{8,6},{9,11},{10,... | collective-permute-start | bytes 1572872 | tf_op jit(solution)/shard_map/ppermute | solution.py:282
  56.9 0.0 copy-done.3
  56.9 3.1 %collective-permute-start.2 = (bf16[2048,128]{1,0:T(8,128)(2,1)S(1)}, bf16[2048,128]{1,0:T(8,128)(2,1)S(1)}, u32[]{:S(2)}, u32[]{:S(2)}) collective-permute-start(bf16[2048,128]{1,0:T(8,128)(2,1)S(1)} %bitcast.22), channel_id=1, source_target_pairs={{0,14},{1,3},{2,0},{3,5},{4,2},{5,7},{6,4},{7,9},{8,6},{9,11},{10,... | collective-permute-start | bytes 1572872 | tf_op jit(solution)/shard_map/ppermute | solution.py:282
  60.1 0.0 copy-done.4
  60.1 3.1 %collective-permute-start.3 = (bf16[128,2048]{1,0:T(8,128)(2,1)S(1)}, bf16[128,2048]{1,0:T(8,128)(2,1)S(1)}, u32[]{:S(2)}, u32[]{:S(2)}) collective-permute-start(bf16[128,2048]{1,0:T(8,128)(2,1)S(1)} %bitcast.24), channel_id=1, source_target_pairs={{0,14},{1,3},{2,0},{3,5},{4,2},{5,7},{6,4},{7,9},{8,6},{9,11},{10,... | collective-permute-start | bytes 1572872 | tf_op jit(solution)/shard_map/ppermute | solution.py:282
  63.2 0.5 shard_map.110.mark_ref
  63.8 1.4 %shard_map.111 = (bf16[192,1024]{1,0:T(8,128)(2,1)S(1)}, bf16[192,1024]{1,0:T(8,128)(2,1)S(1)}, bf16[2048,128]{1,0:T(8,128)(2,1)S(1)}, bf16[2048,128]{1,0:T(8,128)(2,1)S(1)}, bf16[128,2048]{1,0:T(8,128)(2,1)S(1)}) custom-call(bf16[64,48,128]{2,1,0:T(8,128)(2,1)S(1)} %all_to_all.15.wire_ref, f32[8,128]{1,0:T(8,128)S(1)} %shard_map.110.mark_ref, ...), custom_call_target="tpu_custom_call" | custom-call | tf_op jit(solution)/shard_map/pallas_call | solution.py:288
  65.2 0.0 collective-permute-done.1.refs_3_
  65.2 5.4 %collective-permute-done.2.refs_4_ = bf16[2048,128]{1,0:T(8,128)(2,1)S(1)} collective-permute-done((bf16[2048,128]{1,0:T(8,128)(2,1)S(1)}, bf16[2048,128]{1,0:T(8,128)(2,1)S(1)}, u32[]{:S(2)}, u32[]{:S(2)}) %collective-permute-start.2) | collective-permute-done | bytes 524320 | tf_op jit(solution)/shard_map/ppermute | solution.py:282
  70.5 5.6 %collective-permute-done.3.refs_5_ = bf16[128,2048]{1,0:T(8,128)(2,1)S(1)} collective-permute-done((bf16[128,2048]{1,0:T(8,128)(2,1)S(1)}, bf16[128,2048]{1,0:T(8,128)(2,1)S(1)}, u32[]{:S(2)}, u32[]{:S(2)}) %collective-permute-start.3) | collective-permute-done | bytes 524320 | tf_op jit(solution)/shard_map/ppermute | solution.py:282
  76.2 0.0 collective-permute-done.wire_ref
  76.2 3.0 %shard_map.112 = (f32[8,200,128]{2,1,0:T(8,128)S(1)}, bf16[8,200,128]{2,1,0:T(8,128)(2,1)S(1)}, bf16[2,3,192,128]{3,2,1,0:T(8,128)(2,1)S(1)}, bf16[192,1024]{1,0:T(8,128)(2,1)S(1)}, bf16[192,1024]{1,0:T(8,128)(2,1)S(1)}) custom-call(s32[2]{0:T(128)S(1)} %pad_add_fusion.place_ref.core_ref, bf16[192,1024]{1,0:T(8,128)(2,1)S(1)} %get-tuple-element.26.own_t, ...), custom_call_target="tpu_custom_call" | custom-call | tf_op jit(solution)/shard_map/pallas_call | solution.py:293
  79.2 2.3 %collective-permute-start.4 = (bf16[8,200,128]{2,1,0:T(8,128)(2,1)S(1)}, bf16[8,200,128]{2,1,0:T(8,128)(2,1)S(1)}, u32[]{:S(2)}, u32[]{:S(2)}) collective-permute-start(bf16[8,200,128]{2,1,0:T(8,128)(2,1)S(1)} %get-tuple-element.32), channel_id=1, source_target_pairs={{0,1},{1,0},{2,3},{3,2},{4,5},{5,4},{6,7},{7,6},{8,9},{9,8},{10,11... | collective-permute-start | bytes 1228808 | tf_op jit(solution)/shard_map/ppermute | solution.py:37
  81.5 1.4 %collective-permute-done.4 = bf16[8,200,128]{2,1,0:T(8,128)(2,1)S(1)} collective-permute-done((bf16[8,200,128]{2,1,0:T(8,128)(2,1)S(1)}, bf16[8,200,128]{2,1,0:T(8,128)(2,1)S(1)}, u32[]{:S(2)}, u32[]{:S(2)}) %collective-permute-start.4) | collective-permute-done | bytes 409632 | tf_op jit(solution)/shard_map/ppermute | solution.py:37
  82.8 0.9 add_convert_fusion
  83.7 6.5 %all-to-all-start.1 = ((bf16[8,200,128]{2,1,0:T(8,128)(2,1)}), bf16[8,200,128]{2,1,0:T(8,128)(2,1)S(1)}, u32[]{:S(2)}, u32[]{:S(2)}) async-start(bf16[8,200,128]{2,1,0:T(8,128)(2,1)} %add_convert_fusion), calls=%async_computation.1 | async-start | bytes 819200 | tf_op jit(solution)/shard_map/all_to_all | solution.py:300
  90.2 2.3 %shard_map.115 = (bf16[2048,128]{1,0:T(8,128)(2,1)}, bf16[2048,128]{1,0:T(8,128)(2,1)}, bf16[128,2048]{1,0:T(8,128)(2,1)}) custom-call(s32[2]{0:T(128)S(1)} %pad_add_fusion.place_ref.core_ref, bf16[192,1024]{1,0:T(8,128)(2,1)S(1)} %get-tuple-element.26.own_t, bf16[192,1024]{1,0:T(8,128)(2,1)S(1)} %get-tuple-element.35.oth_t, ...), custom_call_target="tpu_custom_call" | custom-call | flops 301989888 | bytes 1572864 | tf_op jit(solution)/shard_map/pallas_call | solution.py:307
  92.5 4.6 %collective-permute-start.5 = (bf16[2048,128]{1,0:T(8,128)(2,1)}, bf16[2048,128]{1,0:T(8,128)(2,1)S(1)}, u32[]{:S(2)}, u32[]{:S(2)}) collective-permute-start(bf16[2048,128]{1,0:T(8,128)(2,1)} %get-tuple-element.41), channel_id=1, source_target_pairs={{14,0},{3,1},{0,2},{5,3},{2,4},{7,5},{4,6},{9,7},{6,8},{11,9},{8,1... | collective-permute-start | bytes 1572872 | tf_op jit(solution)/shard_map/ppermute | solution.py:315
  97.1 3.1 %collective-permute-start.6 = (bf16[2048,128]{1,0:T(8,128)(2,1)}, bf16[2048,128]{1,0:T(8,128)(2,1)S(1)}, u32[]{:S(2)}, u32[]{:S(2)}) collective-permute-start(bf16[2048,128]{1,0:T(8,128)(2,1)} %get-tuple-element.42), channel_id=1, source_target_pairs={{14,0},{3,1},{0,2},{5,3},{2,4},{7,5},{4,6},{9,7},{6,8},{11,9},{8,1... | collective-permute-start | bytes 1572872 | tf_op jit(solution)/shard_map/ppermute | solution.py:315
  100.2 3.1 %collective-permute-start.7 = (bf16[128,2048]{1,0:T(8,128)(2,1)}, bf16[128,2048]{1,0:T(8,128)(2,1)}, u32[]{:S(2)}, u32[]{:S(2)}) collective-permute-start(bf16[128,2048]{1,0:T(8,128)(2,1)} %get-tuple-element.43), channel_id=1, source_target_pairs={{14,0},{3,1},{0,2},{5,3},{2,4},{7,5},{4,6},{9,7},{6,8},{11,9},{8,1... | collective-permute-start | bytes 1572872 | tf_op jit(solution)/shard_map/ppermute | solution.py:315
  103.3 2.4 %all-to-all-done.1.pieces_ref = bf16[8,200,128]{2,1,0:T(8,128)(2,1)S(1)} async-done(((bf16[8,200,128]{2,1,0:T(8,128)(2,1)}), bf16[8,200,128]{2,1,0:T(8,128)(2,1)S(1)}, u32[]{:S(2)}, u32[]{:S(2)}) %all-to-all-start.1) | async-done | bytes 409632 | tf_op jit(solution)/shard_map/all_to_all | solution.py:300
  105.7 1.0 gather.1
  106.7 6.3 %all-to-all-start.2 = ((bf16[64,8,128]{2,1,0:T(8,128)(2,1)}), bf16[64,8,128]{2,1,0:T(8,128)(2,1)S(1)}, u32[]{:S(2)}, u32[]{:S(2)}) async-start(bf16[64,8,128]{2,1,0:T(8,128)(2,1)} %bitcast.8), calls=%async_computation.2 | async-start | bytes 262144 | tf_op jit(solution)/shard_map/all_to_all | solution.py:323
  113.1 1.2 shard_map.114
  114.3 0.0 collective-permute-done.5.refs_3_
  114.3 0.0 collective-permute-done.6.refs_4_
  114.3 4.5 %collective-permute-done.7.refs_5_ = bf16[128,2048]{1,0:T(8,128)(2,1)} collective-permute-done((bf16[128,2048]{1,0:T(8,128)(2,1)}, bf16[128,2048]{1,0:T(8,128)(2,1)}, u32[]{:S(2)}, u32[]{:S(2)}) %collective-permute-start.7) | collective-permute-done | bytes 524320 | tf_op jit(solution)/shard_map/ppermute | solution.py:315
  118.8 2.5 %shard_map.116 = (bf16[2048,128]{1,0:T(8,128)(2,1)}, bf16[2048,128]{1,0:T(8,128)(2,1)}, bf16[128,2048]{1,0:T(8,128)(2,1)}) custom-call(f32[2048,128]{1,0:T(8,128)S(1)} %get-tuple-element.38.refs_0_, f32[2048,128]{1,0:T(8,128)S(1)} %get-tuple-element.39.refs_1_, f32[128,2048]{1,0:T(8,128)S(1)} %get-tuple-element.40.refs_2_, ...), custom_call_target="tpu_custom_call" | custom-call | tf_op jit(solution)/shard_map/pallas_call | solution.py:327
  121.3 3.3 %all-to-all-done.2 = bf16[64,8,128]{2,1,0:T(8,128)(2,1)S(1)} async-done(((bf16[64,8,128]{2,1,0:T(8,128)(2,1)}), bf16[64,8,128]{2,1,0:T(8,128)(2,1)S(1)}, u32[]{:S(2)}, u32[]{:S(2)}) %all-to-all-start.2) | async-done | bytes 131104 | tf_op jit(solution)/shard_map/all_to_all | solution.py:323
  124.6 0.0 copy-start
  124.6 0.0 copy-start.1
  124.6 0.7 copy-done
  125.3 0.0 copy-done.1
  125.3 1.0 shard_map.113
Async XLA Ops:
  3.1 50.7 %copy-start.2 = (bf16[1,2048,128]{2,1,0:T(8,128)(2,1)S(1)}, bf16[1,2048,128]{2,1,0:T(8,128)(2,1)}, u32[]{:S(2)}) copy-start(bf16[1,2048,128]{2,1,0:T(8,128)(2,1)} %param.11) | copy-start | bytes 1572868
  3.1 53.8 %copy-start.3 = (bf16[1,2048,128]{2,1,0:T(8,128)(2,1)S(1)}, bf16[1,2048,128]{2,1,0:T(8,128)(2,1)}, u32[]{:S(2)}) copy-start(bf16[1,2048,128]{2,1,0:T(8,128)(2,1)} %param.12) | copy-start | bytes 1572868
  3.1 57.0 %copy-start.4 = (bf16[1,128,2048]{2,1,0:T(8,128)(2,1)S(1)}, bf16[1,128,2048]{2,1,0:T(8,128)(2,1)}, u32[]{:S(2)}) copy-start(bf16[1,128,2048]{2,1,0:T(8,128)(2,1)} %param.13) | copy-start | bytes 1572868
  49.0 27.2 %collective-permute-start = (bf16[64,48,128]{2,1,0:T(8,128)(2,1)S(1)}, bf16[64,48,128]{2,1,0:T(8,128)(2,1)S(1)}, u32[]{:S(2)}, u32[]{:S(2)}) collective-permute-start(bf16[64,48,128]{2,1,0:T(8,128)(2,1)S(1)} %all_to_all.15.wire_ref), channel_id=1, source_target_pairs={{0,1},{1,0},{2,3},{3,2},{4,5},{5,4},{6,7},{7,6},{8,9},{9,8},{10,11... | collective-permute-start | bytes 2359304 | tf_op jit(solution)/shard_map/ppermute | solution.py:37
  53.8 11.4 %collective-permute-start.1 = (bf16[2048,128]{1,0:T(8,128)(2,1)S(1)}, bf16[2048,128]{1,0:T(8,128)(2,1)S(1)}, u32[]{:S(2)}, u32[]{:S(2)}) collective-permute-start(bf16[2048,128]{1,0:T(8,128)(2,1)S(1)} %bitcast.20), channel_id=1, source_target_pairs={{0,14},{1,3},{2,0},{3,5},{4,2},{5,7},{6,4},{7,9},{8,6},{9,11},{10,... | collective-permute-start | bytes 1572872 | tf_op jit(solution)/shard_map/ppermute | solution.py:282
  56.9 13.6 %collective-permute-start.2 = (bf16[2048,128]{1,0:T(8,128)(2,1)S(1)}, bf16[2048,128]{1,0:T(8,128)(2,1)S(1)}, u32[]{:S(2)}, u32[]{:S(2)}) collective-permute-start(bf16[2048,128]{1,0:T(8,128)(2,1)S(1)} %bitcast.22), channel_id=1, source_target_pairs={{0,14},{1,3},{2,0},{3,5},{4,2},{5,7},{6,4},{7,9},{8,6},{9,11},{10,... | collective-permute-start | bytes 1572872 | tf_op jit(solution)/shard_map/ppermute | solution.py:282
  60.1 16.1 %collective-permute-start.3 = (bf16[128,2048]{1,0:T(8,128)(2,1)S(1)}, bf16[128,2048]{1,0:T(8,128)(2,1)S(1)}, u32[]{:S(2)}, u32[]{:S(2)}) collective-permute-start(bf16[128,2048]{1,0:T(8,128)(2,1)S(1)} %bitcast.24), channel_id=1, source_target_pairs={{0,14},{1,3},{2,0},{3,5},{4,2},{5,7},{6,4},{7,9},{8,6},{9,11},{10,... | collective-permute-start | bytes 1572872 | tf_op jit(solution)/shard_map/ppermute | solution.py:282
  79.2 3.6 %collective-permute-start.4 = (bf16[8,200,128]{2,1,0:T(8,128)(2,1)S(1)}, bf16[8,200,128]{2,1,0:T(8,128)(2,1)S(1)}, u32[]{:S(2)}, u32[]{:S(2)}) collective-permute-start(bf16[8,200,128]{2,1,0:T(8,128)(2,1)S(1)} %get-tuple-element.32), channel_id=1, source_target_pairs={{0,1},{1,0},{2,3},{3,2},{4,5},{5,4},{6,7},{7,6},{8,9},{9,8},{10,11... | collective-permute-start | bytes 1228808 | tf_op jit(solution)/shard_map/ppermute | solution.py:37
  83.7 22.0 %all-to-all-start.1 = ((bf16[8,200,128]{2,1,0:T(8,128)(2,1)}), bf16[8,200,128]{2,1,0:T(8,128)(2,1)S(1)}, u32[]{:S(2)}, u32[]{:S(2)}) async-start(bf16[8,200,128]{2,1,0:T(8,128)(2,1)} %add_convert_fusion), calls=%async_computation.1 | async-start | bytes 819200 | tf_op jit(solution)/shard_map/all_to_all | solution.py:300
  92.5 21.8 %collective-permute-start.5 = (bf16[2048,128]{1,0:T(8,128)(2,1)}, bf16[2048,128]{1,0:T(8,128)(2,1)S(1)}, u32[]{:S(2)}, u32[]{:S(2)}) collective-permute-start(bf16[2048,128]{1,0:T(8,128)(2,1)} %get-tuple-element.41), channel_id=1, source_target_pairs={{14,0},{3,1},{0,2},{5,3},{2,4},{7,5},{4,6},{9,7},{6,8},{11,9},{8,1... | collective-permute-start | bytes 1572872 | tf_op jit(solution)/shard_map/ppermute | solution.py:315
  97.1 17.2 %collective-permute-start.6 = (bf16[2048,128]{1,0:T(8,128)(2,1)}, bf16[2048,128]{1,0:T(8,128)(2,1)S(1)}, u32[]{:S(2)}, u32[]{:S(2)}) collective-permute-start(bf16[2048,128]{1,0:T(8,128)(2,1)} %get-tuple-element.42), channel_id=1, source_target_pairs={{14,0},{3,1},{0,2},{5,3},{2,4},{7,5},{4,6},{9,7},{6,8},{11,9},{8,1... | collective-permute-start | bytes 1572872 | tf_op jit(solution)/shard_map/ppermute | solution.py:315
  100.2 18.6 %collective-permute-start.7 = (bf16[128,2048]{1,0:T(8,128)(2,1)}, bf16[128,2048]{1,0:T(8,128)(2,1)}, u32[]{:S(2)}, u32[]{:S(2)}) collective-permute-start(bf16[128,2048]{1,0:T(8,128)(2,1)} %get-tuple-element.43), channel_id=1, source_target_pairs={{14,0},{3,1},{0,2},{5,3},{2,4},{7,5},{4,6},{9,7},{6,8},{11,9},{8,1... | collective-permute-start | bytes 1572872 | tf_op jit(solution)/shard_map/ppermute | solution.py:315
  106.7 17.9 %all-to-all-start.2 = ((bf16[64,8,128]{2,1,0:T(8,128)(2,1)}), bf16[64,8,128]{2,1,0:T(8,128)(2,1)S(1)}, u32[]{:S(2)}, u32[]{:S(2)}) async-start(bf16[64,8,128]{2,1,0:T(8,128)(2,1)} %bitcast.8), calls=%async_computation.2 | async-start | bytes 262144 | tf_op jit(solution)/shard_map/all_to_all | solution.py:323
  124.6 0.7 copy-start
  124.6 0.7 copy-start.1
